TPU v7x, 256 devices: a whole 4x4x8 slice. The times are simulated.
256 devices in a mesh: fs: 32 (over z, y), tp: 8 (over x, core).
Axes of the slice: x: 4, y: 4, z: 8, core: 2. Of those that a mesh axis runs over, the one named last changes fastest.
Arguments:
- tokens: bfloat16 [65536, 2048], P(('fs', 'tp')), may hold values from -6 to 6
- expert_group: int32 [65536], P(('fs', 'tp')), may hold values from 0 to 7, as said below
- expert_fine: int32 [65536, 2], P(('fs', 'tp')), may hold values from 0 to 3, as said below
- route_weight: float32 [65536, 2], P(('fs', 'tp')), may hold values from 0.2 to 0.9
- norm_gain: float32 [2048], P('fs'), may hold values from 0.1 to 1.9
- gate_master: float32 [32, 2048, 512], P(None, 'fs', 'tp'), may hold values from -0.125 to 0.125
- up_master: float32 [32, 2048, 512], P(None, 'fs', 'tp'), may hold values from -0.125 to 0.125
- down_master: float32 [32, 2048, 512], P(None, 'fs', 'tp'), may hold values from -0.25 to 0.25
Outputs:
- mixed: bfloat16 [65536, 2048], P(('fs', 'tp'))
- gate_ready: bfloat16 [32, 2048, 512], P('fs')
- up_ready: bfloat16 [32, 2048, 512], P('fs')
- down_ready: bfloat16 [32, 2048, 512], P('fs')
Inputs may be any that keep to these rules, and one draw needn't show every extreme that they name: `expert_group`: in the rows of one device every group is chosen by the same number of rows. `expert_fine`: the two entries of a row differ. Counting an expert as its group and entry, the rows of one device name one expert at most 32 times, and in every group one expert is named exactly 32 times by the rows of every device.
All inputs are finite; a program needn't handle non-finite values.
Results may differ from a plain program's by a relative error of at most 0.0086.
Values may be sent and summed in bfloat16 or wider, within the bound.
A program may use at most 128 MiB of HBM per device.

v0:
```python
import jax
import jax.numpy as jnp
from jax import lax
from jax.sharding import PartitionSpec as P

FINE = 4


EPS = 1e-06


def side_by_side(arrays, axis, split_dim, concat_dim, along):
    widths = [a.shape[along] for a in arrays]
    both = jnp.concatenate(arrays, axis=along)
    filled = lax.all_to_all(both, axis, split_axis=split_dim, concat_axis=concat_dim, tiled=True)
    return tuple(jnp.split(filled, [sum(widths[:k]) for k in range(1, len(widths))], axis=along))


def local(
    tokens, expert_group, expert_fine, route_weight, norm_gain, gate_master, up_master, down_master
):
    gate_piece = (norm_gain[None, :, None] * gate_master).astype(jnp.bfloat16)
    up_piece = (norm_gain[None, :, None] * up_master).astype(jnp.bfloat16)
    down_piece = down_master.astype(jnp.bfloat16)
    narrow_cols = side_by_side((gate_piece, up_piece, down_piece), "fs", 0, 1, 2)
    gate_ready, up_ready, down_ready = (
        lax.all_gather(narrow_cols[0], "tp", axis=2, tiled=True),
        lax.all_gather(narrow_cols[1], "tp", axis=2, tiled=True),
        lax.all_gather(narrow_cols[2], "tp", axis=2, tiled=True),
    )
    tok_rows = tokens.shape[0]
    width = tokens.shape[1]
    top_count = expert_fine.shape[1]
    fs_size = lax.axis_size("fs")
    experts_all = gate_master.shape[0]
    local_experts = gate_ready.shape[0]
    capacity = tok_rows // (experts_all // FINE)
    widened = tokens.astype(jnp.float32)
    normed = (
        widened * lax.rsqrt(jnp.mean(widened * widened, axis=-1, keepdims=True) + EPS)
    ).astype(jnp.bfloat16)
    expert = (FINE * expert_group[:, None] + expert_fine).reshape(-1)
    onehot = (expert[:, None] == jnp.arange(experts_all, dtype=jnp.int32)[None, :]).astype(
        jnp.int32
    )
    position = jnp.sum((jnp.cumsum(onehot, axis=0) - onehot) * onehot, axis=1)
    target = expert * capacity + position
    placing = (
        jnp.arange(experts_all * capacity, dtype=jnp.int32)[:, None] == target[None, :]
    ).astype(jnp.bfloat16)
    doubled = jnp.repeat(normed, top_count, axis=0)
    outgoing = jnp.dot(placing, doubled, preferred_element_type=jnp.float32).astype(jnp.bfloat16)
    outgoing = outgoing.reshape(fs_size, local_experts, capacity, width)
    arrived = lax.all_to_all(outgoing, "fs", split_axis=0, concat_axis=0, tiled=True)
    gate_value = jnp.einsum(
        "slcd,ldf->slcf", arrived, gate_ready, preferred_element_type=jnp.float32
    )
    upward = jnp.einsum("slcd,ldf->slcf", arrived, up_ready, preferred_element_type=jnp.float32)
    activation = (jax.nn.silu(gate_value) * upward).astype(jnp.bfloat16)
    expert_out = jnp.einsum(
        "slcf,ldf->slcd", activation, down_ready, preferred_element_type=jnp.float32
    ).astype(jnp.bfloat16)
    returned = lax.all_to_all(expert_out, "fs", split_axis=0, concat_axis=0, tiled=True)
    slotted = returned.reshape(experts_all * capacity, width)
    picked = lax.dot_general(
        placing, slotted, (((0,), (0,)), ((), ())), preferred_element_type=jnp.float32
    )
    picked = picked.reshape(tok_rows, top_count, width)
    mixed = jnp.sum(route_weight[:, :, None] * picked, axis=1).astype(jnp.bfloat16)
    return (mixed, gate_ready, up_ready, down_ready)


def solution(mesh):
    in_specs = (
        P(("fs", "tp"), None),
        P(("fs", "tp")),
        P(("fs", "tp"), None),
        P(("fs", "tp"), None),
        P("fs"),
        P(None, "fs", "tp"),
        P(None, "fs", "tp"),
        P(None, "fs", "tp"),
    )
    out_specs = (
        P(("fs", "tp"), None),
        P("fs", None, None),
        P("fs", None, None),
        P("fs", None, None),
    )
    return jax.shard_map(local, mesh=mesh, in_specs=in_specs, out_specs=out_specs, check_vma=False)
```

profile of v0, /device:TPU:1, one launch (start us, length us, event | category | flops | bytes accessed | tf_op | source)
XLA Modules:
  0.0 290.2 jit_solution(5927202751703197956)
XLA Ops:
  7.2 0.0 copy-start.2
  7.2 1.4 convert_element_type.45
  8.6 0.1 copy-done.2
  8.7 1.6 multiply_convert_fusion.1
  10.3 0.0 copy-start.4
  10.3 0.0 copy-start.3
  10.3 1.5 pad_maximum_fusion
  11.8 12.0 %all-to-all-start = ((bf16[32,64,192]{2,1,0:T(8,128)(2,1)}), bf16[32,64,192]{2,1,0:T(8,128)(2,1)S(1)}, u32[]{:S(2)}, u32[]{:S(2)}) async-start(bf16[32,64,192]{2,1,0:T(8,128)(2,1)} %pad_maximum_fusion), calls=%async_computation | async-start | bytes 2097152 | tf_op jit(solution)/shard_map/all_to_all | solution.py:15
  23.8 0.0 all-gather.6.cloned.1.call-start
  23.9 0.0 copy-done.4
  23.9 0.0 copy-done.3
  23.9 0.1 copy.29
  24.1 0.1 eq.55
  24.2 1.2 reduce-window.6
  25.4 24.6 %all-to-all-done = bf16[32,64,192]{2,1,0:T(8,128)(2,1)S(1)} async-done(((bf16[32,64,192]{2,1,0:T(8,128)(2,1)}), bf16[32,64,192]{2,1,0:T(8,128)(2,1)S(1)}, u32[]{:S(2)}, u32[]{:S(2)}) %all-to-all-start) | async-done | bytes 786464 | tf_op jit(solution)/shard_map/all_to_all | solution.py:15
  50.0 0.0 copy-start
  50.0 1.1 fusion.34
  51.1 1.9 copy.34
  53.1 0.0 all-gather.6.cloned.1.call-update
  53.1 0.2 slice_reduce_fusion
  53.3 0.1 reshape.106
  53.5 0.0 copy-done
  53.5 0.3 fusion.4
  53.8 0.2 fusion.5
  54.1 1.3 broadcast_in_dim.2
  55.3 2.2 reshape.110
  57.5 0.1 fusion.31
  57.7 5.9 %convolution_convert_fusion = bf16[1024,2048]{1,0:T(8,128)(2,1)} fusion(bf16[512,2048]{1,0:T(8,128)(2,1)} %reshape.110, s32[512]{0:T(512)S(1)} %multiply_add_fusion), kind=kOutput, calls=%fused_computation.6 | convolution fusion | flops 2150105088 | bytes 6293504 | tf_op jit(solution)/shard_map/dot_general | solution.py:52
  63.5 6.5 %all-to-all-start.1 = ((bf16[32,1,32,2048]{3,2,1,0:T(8,128)(2,1)}), bf16[32,1,32,2048]{3,2,1,0:T(8,128)(2,1)}, u32[]{:S(2)}, u32[]{:S(2)}) async-start(bf16[32,1,32,2048]{3,2,1,0:T(8,128)(2,1)} %bitcast.100), calls=%async_computation.1 | async-start | bytes 8388608 | tf_op jit(solution)/shard_map/all_to_all | solution.py:54
  70.0 0.0 all-gather.4.cloned.1.call-start
  70.1 0.9 copy.32
  71.0 0.0 all-gather.4.cloned.1.call-update
  71.0 0.2 all-gather.8.cloned.1.call-start
  71.2 0.9 copy.37
  72.1 0.0 all-gather.8.cloned.1.call-update
  72.2 8.5 %all-gather.6.cloned.1.call-done = bf16[1,2048,512]{1,2,0:T(8,128)(2,1)} async-done(((bf16[1,2048,64]{1,2,0:T(8,128)(2,1)}), bf16[1,2048,512]{1,2,0:T(8,128)(2,1)}) %all-gather.6.cloned.1.call-update) | async-done | bytes 2097168 | tf_op jit(solution)/shard_map/all_gather | solution.py:27
  80.7 82.0 %all-to-all-done.1 = bf16[32,1,32,2048]{3,2,1,0:T(8,128)(2,1)} async-done(((bf16[32,1,32,2048]{3,2,1,0:T(8,128)(2,1)}), bf16[32,1,32,2048]{3,2,1,0:T(8,128)(2,1)}, u32[]{:S(2)}, u32[]{:S(2)}) %all-to-all-start.1) | async-done | bytes 4194336 | tf_op jit(solution)/shard_map/all_to_all | solution.py:54
  162.6 5.2 %fusion.2 = f32[512,32,32]{0,2,1:T(8,128)S(1)} fusion(bf16[32,1,32,2048]{3,2,1,0:T(8,128)(2,1)} %all-to-all-done.1, bf16[1,2048,512]{1,2,0:T(8,128)(2,1)} %all-gather.6.cloned.1.call-done), kind=kOutput, calls=%fused_computation.2 | convolution fusion | flops 2147483648 | bytes 8388608 | tf_op jit(solution)/shard_map/slcd,ldf->slcf/dot_general | solution.py:55
  167.8 0.0 all-gather.4.cloned.1.call-done
  167.9 0.0 all-gather.8.cloned.1.call-done
  167.9 10.0 %convert_bitcast_fusion = bf16[32,1,32,2048]{3,2,1,0:T(8,128)(2,1)} fusion(bf16[1,2048,512]{1,2,0:T(8,128)(2,1)} %all-gather.4.cloned.1.call-done, bf16[32,1,32,2048]{3,2,1,0:T(8,128)(2,1)} %all-to-all-done.1, bf16[1,2048,512]{1,2,0:T(8,128)(2,1)} %all-gather.8.cloned.1.call-done, f32[512,32,32]{0,2,1:T(8,128)S(1)} %fusion.2), kind=kOutput, calls=%fused_computation.5 | convolution fusion | flops 4300210176 | bytes 14680064 | tf_op jit(solution)/shard_map/slcf,ldf->slcd/dot_general | solution.py:60
  177.8 7.3 %all-to-all-start.2 = ((bf16[32,1,32,2048]{3,2,1,0:T(8,128)(2,1)}), bf16[32,1,32,2048]{3,2,1,0:T(8,128)(2,1)}, u32[]{:S(2)}, u32[]{:S(2)}) async-start(bf16[32,1,32,2048]{3,2,1,0:T(8,128)(2,1)} %convert_bitcast_fusion), calls=%async_computation.2 | async-start | bytes 8388608 | tf_op jit(solution)/shard_map/all_to_all | solution.py:63
  185.1 0.4 iota_compare_fusion.1
  185.5 1.0 eq.61
  186.5 0.0 copy-start.1
  186.5 4.1 %copy.33 = bf16[1,2048,512]{2,1,0:T(8,128)(2,1)} copy(bf16[1,2048,512]{1,2,0:T(8,128)(2,1)} %all-gather.4.cloned.1.call-done) | data formatting | bytes 4194304 | tf_op jit(solution)/shard_map/all_gather | solution.py:29
  190.6 0.0 copy-done.1
  190.6 2.5 copy.35
  193.0 0.0 copy-start.5
  193.0 3.9 %copy.38 = bf16[1,2048,512]{2,1,0:T(8,128)(2,1)} copy(bf16[1,2048,512]{1,2,0:T(8,128)(2,1)} %all-gather.8.cloned.1.call-done) | data formatting | bytes 4194304 | tf_op jit(solution)/shard_map/all_gather | solution.py:28
  197.0 80.9 %all-to-all-done.2 = bf16[32,1,32,2048]{3,2,1,0:T(8,128)(2,1)} async-done(((bf16[32,1,32,2048]{3,2,1,0:T(8,128)(2,1)}), bf16[32,1,32,2048]{3,2,1,0:T(8,128)(2,1)}, u32[]{:S(2)}, u32[]{:S(2)}) %all-to-all-start.2) | async-done | bytes 4194336 | tf_op jit(solution)/shard_map/all_to_all | solution.py:63
  277.9 0.0 copy-done.5
  277.9 5.8 %multiply_reduce_fusion = bf16[256,2048]{1,0:T(8,128)(2,1)} fusion(bf16[1024,2048,1]{1,0,2:T(8,128)(2,1)} %bitcast.21, f32[256,2]{0,1:T(2,128)S(1)} %copy-done.5, pred[256,2,1024]{2,1,0:T(4,128)(4,1)S(1)} %eq.61), kind=kOutput, calls=%fused_computation.4 | convolution fusion | flops 2149056512 | bytes 5769216 | tf_op jit(solution)/shard_map/dot_general | solution.py:65
  (7 shorter events, 0.1 us)
Async XLA Ops:
  7.2 1.5 copy-start.2
  10.3 13.6 %copy-start.4 = (s32[256]{0:T(256)S(1)}, s32[256]{0:T(256)}, u32[]{:S(2)}) copy-start(s32[256]{0:T(256)} %param.9) | copy-start | bytes 3076
  10.3 13.6 %copy-start.3 = (s32[256,2]{0,1:T(2,128)S(1)}, s32[256,2]{0,1:T(2,128)}, u32[]{:S(2)}) copy-start(s32[256,2]{0,1:T(2,128)} %param.10) | copy-start | bytes 6148
  11.8 38.2 %all-to-all-start = ((bf16[32,64,192]{2,1,0:T(8,128)(2,1)}), bf16[32,64,192]{2,1,0:T(8,128)(2,1)S(1)}, u32[]{:S(2)}, u32[]{:S(2)}) async-start(bf16[32,64,192]{2,1,0:T(8,128)(2,1)} %pad_maximum_fusion), calls=%async_computation | async-start | bytes 2097152 | tf_op jit(solution)/shard_map/all_to_all | solution.py:15
  23.8 56.9 %all-gather.6.cloned.1.call-start = ((), (), s32[]{:S(2)}) async-start(), calls=%async_computation.4 | async-start | bytes 2359296 | tf_op jit(solution)/shard_map/all_gather | solution.py:27
  50.0 3.5 %copy-start = (bf16[256,2048]{1,0:T(8,128)(2,1)S(1)}, bf16[256,2048]{1,0:T(8,128)(2,1)}, u32[]{:S(2)}) copy-start(bf16[256,2048]{1,0:T(8,128)(2,1)} %param.8) | copy-start | bytes 3145732
  63.5 99.1 %all-to-all-start.1 = ((bf16[32,1,32,2048]{3,2,1,0:T(8,128)(2,1)}), bf16[32,1,32,2048]{3,2,1,0:T(8,128)(2,1)}, u32[]{:S(2)}, u32[]{:S(2)}) async-start(bf16[32,1,32,2048]{3,2,1,0:T(8,128)(2,1)} %bitcast.100), calls=%async_computation.1 | async-start | bytes 8388608 | tf_op jit(solution)/shard_map/all_to_all | solution.py:54
  70.0 97.8 %all-gather.4.cloned.1.call-start = ((), (), s32[]{:S(2)}) async-start(), calls=%async_computation.3 | async-start | bytes 2359296 | tf_op jit(solution)/shard_map/all_gather | solution.py:29
  71.0 96.9 %all-gather.8.cloned.1.call-start = ((), (), s32[]{:S(2)}) async-start(), calls=%async_computation.5 | async-start | bytes 2359296 | tf_op jit(solution)/shard_map/all_gather | solution.py:28
  177.8 100.0 %all-to-all-start.2 = ((bf16[32,1,32,2048]{3,2,1,0:T(8,128)(2,1)}), bf16[32,1,32,2048]{3,2,1,0:T(8,128)(2,1)}, u32[]{:S(2)}, u32[]{:S(2)}) async-start(bf16[32,1,32,2048]{3,2,1,0:T(8,128)(2,1)} %convert_bitcast_fusion), calls=%async_computation.2 | async-start | bytes 8388608 | tf_op jit(solution)/shard_map/all_to_all | solution.py:63
  186.5 4.1 %copy-start.1 = (bf16[1,2048,512]{1,2,0:T(8,128)(2,1)S(1)}, bf16[1,2048,512]{1,2,0:T(8,128)(2,1)}, u32[]{:S(2)}) copy-start(bf16[1,2048,512]{1,2,0:T(8,128)(2,1)} %all-gather.6.cloned.1.call-done) | copy-start | bytes 6291460
  193.0 84.8 %copy-start.5 = (f32[256,2]{0,1:T(2,128)S(1)}, f32[256,2]{0,1:T(2,128)}, u32[]{:S(2)}) copy-start(f32[256,2]{0,1:T(2,128)} %param.11) | copy-start | bytes 6148
Sparse Core Ops, SparseCore 0:
  53.2 27.4 all-gather.5
  83.1 28.2 all-gather.3
  113.8 28.2 all-gather.7
where the time goes:
time: 293 us; the launch traced here: 290 us
  waiting for transfers between devices  196 us (67%)
  matrix products  26.8 us (9%)
  starting transfers between devices  26.1 us (9%)
  local copies, waits for them, and re-layouts  20.6 us (7%)
  between operations  13.9 us (5%)
  other arithmetic  6.65 us (2%)
    all_to_all x1, waiting for transfers between devices, local(): lax.all_to_all(outgoing, 'fs', split_axis=0, concat_axis=0, tiled=True)  82 us
    all_to_all x1, waiting for transfers between devices, local(): lax.all_to_all(expert_out, 'fs', split_axis=0, concat_axis=0, tiled=True)  80.9 us
    all_to_all x1, waiting for transfers between devices, side_by_side(): lax.all_to_all(both, axis, split_axis=split_dim, concat_axis=concat_dim,...  24.6 us
    all_to_all x1, starting transfers between devices, side_by_side(): lax.all_to_all(both, axis, split_axis=split_dim, concat_axis=concat_dim,...  12 us
    dot_general x1, matrix products, local(): jnp.einsum('slcf,ldf->slcd', activation, down_ready, preferred_element_ty...  9.96 us
    all_gather x1, waiting for transfers between devices, local(): lax.all_gather(narrow_cols[0], 'tp', axis=2, tiled=True)  8.52 us
    all_to_all x1, starting transfers between devices, local(): lax.all_to_all(expert_out, 'fs', split_axis=0, concat_axis=0, tiled=True)  7.28 us
    all_to_all x1, starting transfers between devices, local(): lax.all_to_all(outgoing, 'fs', split_axis=0, concat_axis=0, tiled=True)  6.51 us
  transfers between devices with their start and end apart: 6, of which 4 were waited for; matrix products, arithmetic and copies ran while one was open for 11% of the time, Pallas kernels for 0%

commit v1 on v0

v1 whole, which is shorter than its diff:
```python
import jax
import jax.numpy as jnp
from jax import lax
from jax.sharding import Mesh, PartitionSpec as P

FINE = 4
EPS = 1e-06
BF = jnp.bfloat16


def exchange_weights(gate_piece, up_piece, down_piece):
    both = jnp.concatenate((gate_piece, up_piece, down_piece), axis=2)
    filled = lax.all_to_all(both, ("z", "y"), split_axis=0, concat_axis=1, tiled=True)
    parts = jnp.split(filled, 3, axis=2)
    return tuple(lax.all_gather(a, ("x", "c"), axis=2, tiled=True) for a in parts)


def local(
    tokens, expert_group, expert_fine, route_weight, norm_gain, gate_master, up_master, down_master
):
    gate_piece = (norm_gain[None, :, None] * gate_master).astype(BF)
    up_piece = (norm_gain[None, :, None] * up_master).astype(BF)
    down_piece = down_master.astype(BF)
    gate_ready, up_ready, down_ready = exchange_weights(gate_piece, up_piece, down_piece)

    rows, width = tokens.shape
    groups = lax.axis_size("z")
    per_group = rows // groups
    widened = tokens.astype(jnp.float32)
    normed = (
        widened * lax.rsqrt(jnp.mean(widened * widened, axis=-1, keepdims=True) + EPS)
    ).astype(BF)
    same = (expert_group[:, None] == jnp.arange(groups)[None, :]).astype(BF)
    ahead = jnp.arange(rows)[:, None] > jnp.arange(rows)[None, :]
    before = jnp.dot(ahead.astype(BF), same, preferred_element_type=jnp.float32)
    position = jnp.sum(before * same.astype(jnp.float32), axis=1).astype(jnp.int32)
    slot = expert_group * per_group + position
    placing = (jnp.arange(rows, dtype=jnp.int32)[:, None] == slot[None, :]).astype(BF)
    fine_weight = jnp.sum(
        jnp.where(
            expert_fine[:, :, None] == jnp.arange(FINE)[None, None, :],
            route_weight[:, :, None],
            0.0,
        ),
        axis=1,
    )
    high = fine_weight.astype(BF)
    rest = fine_weight - high.astype(jnp.float32)
    low = rest.astype(BF)
    packed = jnp.concatenate(
        (normed, high, low, jnp.zeros((rows, 128 - 2 * FINE), BF)), axis=1
    )
    outgoing = jnp.dot(placing, packed, preferred_element_type=jnp.float32).astype(BF)
    outgoing = outgoing.reshape(groups, per_group, width + 128)
    arrived = lax.all_to_all(outgoing, "z", split_axis=0, concat_axis=0, tiled=True)
    gathered = lax.all_gather(arrived, "y", axis=0, tiled=False)
    gathered = gathered.reshape(FINE * rows, width + 128)
    data = gathered[:, :width]
    mine = lax.axis_index("y")
    pick = (jnp.arange(FINE) == mine).astype(jnp.float32)[None, :]
    scale = jnp.sum(
        pick
        * (
            gathered[:, width : width + FINE].astype(jnp.float32)
            + gathered[:, width + FINE : width + 2 * FINE].astype(jnp.float32)
        ),
        axis=1,
        keepdims=True,
    )
    gate_value = jnp.dot(data, gate_ready[0], preferred_element_type=jnp.float32)
    upward = jnp.dot(data, up_ready[0], preferred_element_type=jnp.float32)
    activation = (jax.nn.silu(gate_value) * upward).astype(BF)
    out = lax.dot_general(
        activation, down_ready[0], (((1,), (1,)), ((), ())), preferred_element_type=jnp.float32
    )
    out = (out.astype(BF).astype(jnp.float32) * scale).astype(BF)
    summed = lax.psum_scatter(out, "y", scatter_dimension=0, tiled=True)
    back = lax.all_to_all(
        summed.reshape(groups, per_group, width), "z", split_axis=0, concat_axis=0, tiled=True
    )
    mixed = lax.dot_general(
        placing,
        back.reshape(rows, width),
        (((0,), (0,)), ((), ())),
        preferred_element_type=jnp.float32,
    ).astype(BF)
    return (mixed, gate_ready, up_ready, down_ready)


def solution(mesh):
    fine = Mesh(mesh.devices.reshape(8, 4, 4, 2), ("z", "y", "x", "c"))
    fs, tp = ("z", "y"), ("x", "c")
    token = fs + tp
    in_specs = (
        P(token, None),
        P(token),
        P(token, None),
        P(token, None),
        P(fs),
        P(None, fs, tp),
        P(None, fs, tp),
        P(None, fs, tp),
    )
    out_specs = (
        P(token, None),
        P(fs, None, None),
        P(fs, None, None),
        P(fs, None, None),
    )
    return jax.shard_map(local, mesh=fine, in_specs=in_specs, out_specs=out_specs, check_vma=False)
```

time: 293 us -> 307 us (1.048)
  blocking collectives: 0 us -> 69.6 us
  starting transfers between devices: 26.1 us -> 6.94 us
  waiting for transfers between devices: 196 us -> 177 us
  matrix products: 26.8 us -> 18.3 us
  local copies, waits for them, and re-layouts: 20.6 us -> 15.1 us
    all_to_all x3 -> x1, waiting for transfers between devices: 187 us -> 20.1 us  [local(): lax.all_to_all(summed.reshape(groups, per_group, width), 'z', split_axis=...]
    all_gather x3 -> x4, waiting for transfers between devices: 8.55 us -> 107 us  [the longest x3 83.1 us: exchange_weights(): lax.all_gather(a, ('x', 'c'), axis=2, tiled=True)]
    all_to_all x0 -> x2, blocking collectives: none -> 69.6 us  [the longest x1 38.2 us: local(): lax.all_to_all(outgoing, 'z', split_axis=0, concat_axis=0, tiled=True)]
    reduce_scatter x0 -> x1, waiting for transfers between devices: none -> 49.5 us  [local(): summed = lax.psum_scatter(out, 'y', scatter_dimension=0, tiled=True)]
    all_to_all x3 -> x1, starting transfers between devices: 25.8 us -> 6.73 us  [local(): lax.all_to_all(summed.reshape(groups, per_group, width), 'z', split_axis=...]
    all_gather x3 -> x0, local copies, waits for them, and re-layouts: 10.5 us -> none  [the longest x1 4.07 us: local(): lax.all_gather(narrow_cols[2], 'tp', axis=2, tiled=True)]
    unnamed x12 -> x17, local copies, waits for them, and re-layouts: 0.16 us -> 9.37 us
    dot_general x4 -> x5, matrix products: 26.8 us -> 18.3 us  [the longest x1 10.2 us: local(): lax.dot_general(activation, down_ready[0], (((1,), (1,)), ((), ())), pref...]
  transfers between devices with their start and end apart: 6 -> 6, of which waited for: 4 -> 6; matrix products, arithmetic and copies ran while one was open for 11% -> 7% of each run, Pallas kernels for 0% -> 0%
where the time goes in v1:
time: 307 us; the launch traced here: 306 us
  waiting for transfers between devices  177 us (58%)
  blocking collectives  69.6 us (23%)
  matrix products  18.3 us (6%)
  local copies, waits for them, and re-layouts  15.1 us (5%)
  between operations  14 us (5%)
  starting transfers between devices  6.94 us (2%)
  other arithmetic  5.42 us (2%)
    all_gather x3, waiting for transfers between devices, exchange_weights(): lax.all_gather(a, ('x', 'c'), axis=2, tiled=True)  83.1 us
    reduce_scatter x1, waiting for transfers between devices, local(): summed = lax.psum_scatter(out, 'y', scatter_dimension=0, tiled=True)  49.5 us
    all_to_all x1, blocking collectives, local(): lax.all_to_all(outgoing, 'z', split_axis=0, concat_axis=0, tiled=True)  38.2 us
    all_to_all x1, blocking collectives, exchange_weights(): lax.all_to_all(both, ('z', 'y'), split_axis=0, concat_axis=1, tiled=True)  31.4 us
    all_gather x1, waiting for transfers between devices, local(): gathered = lax.all_gather(arrived, 'y', axis=0, tiled=False)  24.2 us
    all_to_all x1, waiting for transfers between devices, local(): lax.all_to_all(summed.reshape(groups, per_group, width), 'z', split_axis=...  20.1 us
    dot_general x1, matrix products, local(): lax.dot_general(activation, down_ready[0], (((1,), (1,)), ((), ())), pref...  10.2 us
    unnamed x17, local copies, waits for them, and re-layouts  9.37 us
  transfers between devices with their start and end apart: 6, of which 6 were waited for; matrix products, arithmetic and copies ran while one was open for 7% of the time, Pallas kernels for 0%

profile of v1, /device:TPU:1, one launch (start us, length us, event | category | flops | bytes accessed | tf_op | source)
XLA Modules:
  0.0 306.3 jit_solution(3773727726273572708)
XLA Ops:
  7.2 0.0 all-gather.12.cloned.1.call-start
  7.2 1.5 fusion.4
  8.7 1.0 fusion.13
  9.7 0.7 convert_add_fusion
  10.4 0.7 select_reduce_fusion
  11.1 0.1 copy.46
  11.2 0.1 copy.45
  11.4 1.5 fusion.5
  12.9 1.0 concatenate.6
  13.9 0.5 convolution_convert_fusion
  14.4 0.0 copy-start.2
  14.4 0.0 copy-start.3
  14.4 0.0 copy-start.4
  14.4 0.0 copy-start.5
  14.5 38.2 %all_to_all.22 = bf16[8,32,2176]{2,1,0:T(8,128)(2,1)} all-to-all(bf16[8,32,2176]{2,1,0:T(8,128)(2,1)S(1)} %bitcast.21), channel_id=1, replica_groups=mesh['z'=8,'y'=4,'x'=4,'c'=2] {'z'}, dimensions={0} | all-to-all | bytes 2228224 | tf_op jit(solution)/shard_map/all_to_all | solution.py:55
  52.6 0.0 all-gather.12.cloned.1.call-update
  52.6 0.0 all-gather.6.cloned.1.call-start
  52.7 0.0 copy-done.2
  52.7 0.1 convert_element_type.77
  52.8 0.0 copy-done.3
  52.8 0.0 copy-done.4
  52.8 0.0 copy-done.5
  52.8 0.3 multiply_convert_fusion.3
  53.2 0.5 pad_maximum_fusion
  53.7 31.4 %all_to_all.23 = bf16[32,64,192]{2,1,0:T(8,128)(2,1)S(1)} all-to-all(bf16[32,64,192]{2,1,0:T(8,128)(2,1)S(1)} %pad_maximum_fusion), channel_id=1, replica_groups=mesh['z'=8,'y'=4,'x'=4,'c'=2] {'z','y'}, dimensions={0} | all-to-all | bytes 1572864 | tf_op jit(solution)/shard_map/all_to_all | solution.py:13
  85.1 0.3 fusion.24
  85.5 0.9 copy.47
  86.4 0.0 all-gather.6.cloned.1.call-update
  86.4 0.0 all-gather.8.cloned.1.call-start
  86.4 0.9 copy.48
  87.3 0.0 all-gather.8.cloned.1.call-update
  87.4 0.0 all-gather.10.cloned.1.call-start
  87.4 0.9 copy.49
  88.3 0.0 all-gather.10.cloned.1.call-update
  88.3 0.0 reduce-scatter.2.cloned.1.call-start
  88.4 24.2 %all-gather.12.cloned.1.call-done = bf16[32,32,2176]{2,1,0:T(8,128)(2,1)} async-done(((bf16[8,32,2176]{2,1,0:T(8,128)(2,1)}), bf16[32,32,2176]{2,1,0:T(8,128)(2,1)}) %all-gather.12.cloned.1.call-update) | async-done | bytes 4456464 | tf_op jit(solution)/shard_map/all_gather | solution.py:56
  112.6 1.4 fusion.23
  114.0 0.1 copy.55
  114.1 0.1 copy.56
  114.3 0.1 multiply_reduce_fusion
  114.4 27.0 %all-gather.6.cloned.1.call-done = bf16[1,2048,512]{1,2,0:T(8,128)(2,1)} async-done(((bf16[1,2048,64]{1,2,0:T(8,128)(2,1)}), bf16[1,2048,512]{1,2,0:T(8,128)(2,1)}) %all-gather.6.cloned.1.call-update) | async-done | bytes 2097168 | tf_op jit(solution)/shard_map/all_gather | solution.py:15
  141.3 5.2 %fusion.2 = f32[1024,512]{1,0:T(8,128)S(1)} fusion(bf16[1024,2176]{1,0:T(8,128)(2,1)} %bitcast.25, bf16[1,2048,512]{1,2,0:T(8,128)(2,1)} %all-gather.6.cloned.1.call-done), kind=kOutput, calls=%fused_computation.4 | convolution fusion | flops 2147483648 | bytes 8388608 | tf_op jit(solution)/shard_map/dot_general | solution.py:70
  146.6 25.5 %all-gather.8.cloned.1.call-done = bf16[1,2048,512]{1,2,0:T(8,128)(2,1)} async-done(((bf16[1,2048,64]{1,2,0:T(8,128)(2,1)}), bf16[1,2048,512]{1,2,0:T(8,128)(2,1)}) %all-gather.8.cloned.1.call-update) | async-done | bytes 2097168 | tf_op jit(solution)/shard_map/all_gather | solution.py:15
  172.1 30.6 %all-gather.10.cloned.1.call-done = bf16[1,2048,512]{1,2,0:T(8,128)(2,1)} async-done(((bf16[1,2048,64]{1,2,0:T(8,128)(2,1)}), bf16[1,2048,512]{1,2,0:T(8,128)(2,1)}) %all-gather.10.cloned.1.call-update) | async-done | bytes 2097168 | tf_op jit(solution)/shard_map/all_gather | solution.py:15
  202.6 10.2 %multiply_convert_fusion = bf16[1024,2048]{1,0:T(8,128)(2,1)} fusion(f32[1024]{0:T(1024)S(1)} %multiply_reduce_fusion, bf16[1,2048,512]{1,2,0:T(8,128)(2,1)} %all-gather.10.cloned.1.call-done, f32[1024,512]{1,0:T(8,128)S(1)} %fusion.2, bf16[1,2048,512]{1,2,0:T(8,128)(2,1)} %all-gather.8.cloned.1.call-done, bf16[1024,2176]{1,0:T(8,128)(2,1)} %bitcast.26), kind=kOutput, calls=%fused_computation | convolution fusion | flops 4306501632 | bytes 14684160 | tf_op jit(solution)/shard_map/dot_general | solution.py:73
  212.8 0.0 reduce-scatter.2.cloned.1.call-update
  212.8 0.0 copy-start
  212.8 49.5 %reduce-scatter.2.cloned.1.call-done = bf16[256,2048]{1,0:T(8,128)(2,1)} async-done(((bf16[1024,2048]{1,0:T(8,128)(2,1)}), bf16[256,2048]{1,0:T(8,128)(2,1)}) %reduce-scatter.2.cloned.1.call-update) | async-done | bytes 1048592 | tf_op jit(solution)/shard_map/reduce_scatter | solution.py:77
  262.4 6.7 %all-to-all-start.2 = ((bf16[8,32,2048]{2,1,0:T(8,128)(2,1)}), bf16[8,32,2048]{2,1,0:T(8,128)(2,1)S(1)}, u32[]{:S(2)}, u32[]{:S(2)}) async-start(bf16[8,32,2048]{2,1,0:T(8,128)(2,1)} %bitcast.23), calls=%async_computation.3 | async-start | bytes 2097152 | tf_op jit(solution)/shard_map/all_to_all | solution.py:78
  269.1 0.0 copy-done
  269.1 2.5 copy.52
  271.6 0.0 copy-start.1
  271.6 4.1 %copy.53 = bf16[1,2048,512]{2,1,0:T(8,128)(2,1)} copy(bf16[1,2048,512]{1,2,0:T(8,128)(2,1)} %all-gather.8.cloned.1.call-done) | data formatting | bytes 4194304
  275.7 0.0 copy-done.1
  275.7 2.5 copy.54
  278.2 20.1 %all-to-all-done.2 = bf16[8,32,2048]{2,1,0:T(8,128)(2,1)S(1)} async-done(((bf16[8,32,2048]{2,1,0:T(8,128)(2,1)}), bf16[8,32,2048]{2,1,0:T(8,128)(2,1)S(1)}, u32[]{:S(2)}, u32[]{:S(2)}) %all-to-all-start.2) | async-done | bytes 1048608 | tf_op jit(solution)/shard_map/all_to_all | solution.py:78
  298.3 1.5 convolution_convert_fusion.1
  (4 shorter events, 0.0 us)
Async XLA Ops:
  7.2 105.4 %all-gather.12.cloned.1.call-start = ((), (), s32[]{:S(2)}) async-start(), calls=%async_computation.8 | async-start | bytes 5570560 | tf_op jit(solution)/shard_map/all_gather | solution.py:56
  14.4 38.3 %copy-start.2 = (f32[32,64,64]{2,1,0:T(8,128)S(1)}, f32[32,64,64]{2,1,0:T(8,128)}, u32[]{:S(2)}) copy-start(f32[32,64,64]{2,1,0:T(8,128)} %param.15) | copy-start | bytes 1572868
  14.4 38.4 %copy-start.3 = (f32[32,64,64]{2,1,0:T(8,128)S(1)}, f32[32,64,64]{2,1,0:T(8,128)}, u32[]{:S(2)}) copy-start(f32[32,64,64]{2,1,0:T(8,128)} %param.13) | copy-start | bytes 1572868
  14.4 38.4 %copy-start.4 = (f32[32,64,64]{2,1,0:T(8,128)S(1)}, f32[32,64,64]{2,1,0:T(8,128)}, u32[]{:S(2)}) copy-start(f32[32,64,64]{2,1,0:T(8,128)} %param.14) | copy-start | bytes 1572868
  14.4 38.4 %copy-start.5 = (f32[64]{0:T(128)S(1)}, f32[64]{0:T(128)}, u32[]{:S(2)}) copy-start(f32[64]{0:T(128)} %param.12) | copy-start | bytes 772
  52.6 88.7 %all-gather.6.cloned.1.call-start = ((), (), s32[]{:S(2)}) async-start(), calls=%async_computation.4 | async-start | bytes 2359296 | tf_op jit(solution)/shard_map/all_gather | solution.py:15
  86.4 85.7 %all-gather.8.cloned.1.call-start = ((), (), s32[]{:S(2)}) async-start(), calls=%async_computation.5 | async-start | bytes 2359296 | tf_op jit(solution)/shard_map/all_gather | solution.py:15
  87.4 115.3 %all-gather.10.cloned.1.call-start = ((), (), s32[]{:S(2)}) async-start(), calls=%async_computation.6 | async-start | bytes 2359296 | tf_op jit(solution)/shard_map/all_gather | solution.py:15
  88.3 174.0 %reduce-scatter.2.cloned.1.call-start = ((), (), s32[]{:S(2)}) async-start(), calls=%async_computation.7 | async-start | bytes 5242880 | tf_op jit(solution)/shard_map/reduce_scatter | solution.py:77
  212.8 56.3 %copy-start = (bf16[1,2048,512]{1,2,0:T(8,128)(2,1)S(1)}, bf16[1,2048,512]{1,2,0:T(8,128)(2,1)}, u32[]{:S(2)}) copy-start(bf16[1,2048,512]{1,2,0:T(8,128)(2,1)} %all-gather.6.cloned.1.call-done) | copy-start | bytes 6291460
  262.4 35.9 %all-to-all-start.2 = ((bf16[8,32,2048]{2,1,0:T(8,128)(2,1)}), bf16[8,32,2048]{2,1,0:T(8,128)(2,1)S(1)}, u32[]{:S(2)}, u32[]{:S(2)}) async-start(bf16[8,32,2048]{2,1,0:T(8,128)(2,1)} %bitcast.23), calls=%async_computation.3 | async-start | bytes 2097152 | tf_op jit(solution)/shard_map/all_to_all | solution.py:78
  271.6 4.1 %copy-start.1 = (bf16[1,2048,512]{1,2,0:T(8,128)(2,1)S(1)}, bf16[1,2048,512]{1,2,0:T(8,128)(2,1)}, u32[]{:S(2)}) copy-start(bf16[1,2048,512]{1,2,0:T(8,128)(2,1)} %all-gather.10.cloned.1.call-done) | copy-start | bytes 6291460
Sparse Core Ops, SparseCore 0:
  52.8 59.7 all-gather.11
  115.0 26.2 all-gather.5
  143.8 28.2 all-gather.7
  174.4 28.2 all-gather.9
  213.0 49.3 reduce-scatter.1

commit v2 on v1

v2 whole, which is shorter than its diff:
```python
import jax
import jax.numpy as jnp
from jax import lax
from jax.experimental import pallas as pl
from jax.experimental.pallas import tpu as pltpu
from jax.sharding import Mesh, PartitionSpec as P

FINE = 4
EPS = 1e-06
BF = jnp.bfloat16
F32 = jnp.float32
NZ, NY, NX = 8, 4, 4
ROWS = 32
HALF = 16
D = 2048
LANE = 128
WIDE = D + LANE
MESH = pl.DeviceIdType.MESH


def offset_of(s):
    far = (s + 1) // 2
    odd = s % 2
    return (odd * far + (1 - odd) * (NZ - far)) % NZ


def kernel(
    rows_in, pieces, back_out, gate_out, up_out, down_out,
    a, o, h, f, zsum, back, w, wsend, wz, other,
    zt_s, zt_r, zw_s, zw_r, ag_s, ag_r, yw_s, yw_r, xw_s, xw_r, cw_s, cw_r,
    pair_s, pair_r, rs_s, rs_r, zb_s, zb_r, out_sem, back_sem,
):
    z, y, x, c = (lax.axis_index(n) for n in ("z", "y", "x", "c"))
    yp, ym = (y + 1) % NY, (y + NY - 1) % NY
    xp, xm = (x + 1) % NX, (x + NX - 1) % NX

    def remote(src, dst, ss, rs, where):
        return pltpu.make_async_remote_copy(
            src_ref=src, dst_ref=dst, send_sem=ss, recv_sem=rs,
            device_id=where, device_id_type=MESH,
        )

    def to_z(s):
        return (z + offset_of(s)) % NZ

    def from_z(s):
        return (z + NZ - offset_of(s)) % NZ

    def zt(s):
        return remote(rows_in.at[to_z(s)], a.at[s, 0], zt_s.at[s], zt_r.at[s], {"z": to_z(s)})

    def zw(s):
        return remote(
            wsend.at[pl.ds(FINE * to_z(s), FINE)], wz.at[s], zw_s.at[s], zw_r.at[s], {"z": to_z(s)}
        )

    def ag(s, j):
        if j == 0:
            src = rows_in.at[z] if isinstance(s, int) and s == 0 else a.at[s, 0]
            dst, where = a.at[s, 1], yp
        elif j == 1:
            src = rows_in.at[z] if isinstance(s, int) and s == 0 else a.at[s, 0]
            dst, where = a.at[s, 3], ym
        elif j == 2:
            src, dst, where = a.at[s, 1, pl.ds(0, HALF)], a.at[s, 2, pl.ds(0, HALF)], yp
        else:
            src, dst, where = a.at[s, 3, pl.ds(HALF, HALF)], a.at[s, 2, pl.ds(HALF, HALF)], ym
        return remote(src, dst, ag_s.at[s, j], ag_r.at[s, j], {"y": where})

    def yw(s, k):
        t = (y + k) % NY
        src = wsend.at[FINE * z + t] if isinstance(s, int) and s == 0 else wz.at[s, t]
        dst = w.at[:, x, NY * from_z(s) + y, c]
        return remote(src, dst, yw_s.at[s, k - 1], yw_r.at[s, k - 1], {"y": t})

    def xw(s, j):
        base = NY * from_z(s)
        if j == 0:
            part, where = w.at[:, x, pl.ds(base, NY), c], xp
        elif j == 1:
            part, where = w.at[:, x, pl.ds(base, NY), c], xm
        elif j == 2:
            part, where = w.at[:, xm, pl.ds(base, 2), c], xp
        else:
            part, where = w.at[:, xp, pl.ds(base + 2, 2), c], xm
        return remote(part, part, xw_s.at[s, j], xw_r.at[s, j], {"x": where})

    def cw(s):
        part = w.at[:, :, pl.ds(NY * from_z(s), NY), c]
        return remote(part, part, cw_s.at[s], cw_r.at[s], {"c": 1 - c})

    def rs(s, j):
        if j == 0:
            src, dst, where = o.at[s, 2, pl.ds(0, HALF)], h.at[s, 0], ym
        elif j == 1:
            src, dst, where = o.at[s, 2, pl.ds(HALF, HALF)], h.at[s, 1], yp
        elif j == 2:
            src, dst, where = o.at[s, 1], f.at[s, 0], ym
        else:
            src, dst, where = o.at[s, 3], f.at[s, 1], yp
        return remote(src, dst, rs_s.at[s, j], rs_r.at[s, j], {"y": where})

    def zb(s):
        return remote(zsum.at[s], back.at[z], zb_s.at[s], zb_r.at[s], {"z": from_z(s)})

    def w_a(s):
        if isinstance(s, int) and s == 0:
            mine = wsend[FINE * z + y]
        else:
            zw(s).wait_recv()
            mine = wz[s, y]
        for k in (1, 3, 2):
            yw(s, k).start()
        w[:, x, NY * from_z(s) + y, c] = mine

    def w_b(s):
        for k in (1, 3, 2):
            yw(s, k).wait_recv()
        xw(s, 0).start()
        xw(s, 1).start()

    def w_c(s):
        xw(s, 0).wait_recv()
        xw(s, 2).start()
        xw(s, 1).wait_recv()
        xw(s, 3).start()

    def w_d(s):
        xw(s, 2).wait_recv()
        xw(s, 3).wait_recv()
        cw(s).start()

    def t_a(s):
        if not (isinstance(s, int) and s == 0):
            zt(s).wait_recv()
        ag(s, 0).start()
        ag(s, 1).start()

    def t_b(s):
        ag(s, 0).wait_recv()
        ag(s, 2).start()
        ag(s, 1).wait_recv()
        ag(s, 3).start()

    def expert(s):
        data = a[s, :, :, 0:D].reshape(NY * ROWS, D)
        extra = a[s, :, :, D:WIDE].reshape(NY * ROWS, LANE).astype(F32)
        lane = lax.broadcasted_iota(jnp.int32, (NY * ROWS, LANE), 1)
        chosen = (lane == y) | (lane == y + FINE)
        scale = jnp.sum(jnp.where(chosen, extra, 0.0), axis=1, keepdims=True)
        acts = []
        for xb in range(NX):
            both = jnp.concatenate(
                [w[0, xb].reshape(D, LANE), w[1, xb].reshape(D, LANE)], axis=1
            )
            r = jnp.dot(data, both, preferred_element_type=F32)
            g, u = r[:, :LANE], r[:, LANE:]
            acts.append((g / (1.0 + jnp.exp(-g)) * u).astype(BF))
        act = jnp.concatenate(acts, axis=1)
        for nb in range(8):
            rhs = jnp.concatenate(
                [w[2, xb, 4 * nb : 4 * nb + 4].reshape(256, LANE) for xb in range(NX)], axis=1
            )
            r = lax.dot_general(
                act, rhs, (((1,), (1,)), ((), ())), preferred_element_type=F32
            )
            r = (r.astype(BF).astype(F32) * scale).astype(BF)
            o[s, :, :, 256 * nb : 256 * nb + 256] = r.reshape(NY, ROWS, 256)

    def t_c(s):
        ag(s, 2).wait_recv()
        ag(s, 3).wait_recv()
        expert(s)
        rs(s, 0).start()
        rs(s, 1).start()

    def t_d(s):
        rs(s, 0).wait_recv()
        o[s, 1, 0:HALF] = (o[s, 1, 0:HALF].astype(F32) + h[s, 0].astype(F32)).astype(BF)
        rs(s, 2).start()
        rs(s, 1).wait_recv()
        o[s, 3, HALF:ROWS] = (o[s, 3, HALF:ROWS].astype(F32) + h[s, 1].astype(F32)).astype(BF)
        rs(s, 3).start()

    def total(s):
        rs(s, 2).wait_recv()
        rs(s, 3).wait_recv()
        return (o[s, 0].astype(F32) + f[s, 0].astype(F32) + f[s, 1].astype(F32)).astype(BF)

    def t_e(s):
        zsum[s] = total(s)
        zb(s).start()

    barrier = pltpu.get_barrier_semaphore()
    peers = (
        [{"z": (z + k) % NZ} for k in range(1, NZ)]
        + [{"y": (y + k) % NY} for k in range(1, NY)]
        + [{"x": (x + k) % NX} for k in range(1, NX)]
        + [{"c": 1 - c}]
    )
    for peer in peers:
        pl.semaphore_signal(barrier, inc=1, device_id=peer, device_id_type=MESH)
    pl.semaphore_wait(barrier, len(peers))

    pair = remote(pieces.at[:, 1 - c], other, pair_s, pair_r, {"c": 1 - c})
    pair.start()
    zt(1).start()
    zt(2).start()
    t_a(0)
    a[0, 0] = rows_in[z]
    pair.wait_recv()

    def join(e, carry):
        mine, theirs = pieces[e, c], other[e]
        low = jnp.where(c == 0, mine, theirs)
        high = jnp.where(c == 0, theirs, mine)
        wsend[e] = jnp.concatenate([low, high], axis=-1)
        return carry

    lax.fori_loop(0, NZ * FINE, join, 0)

    def send_w(s, carry):
        zw(s).start()
        return carry

    lax.fori_loop(1, NZ, send_w, 0)

    def send_t(s, carry):
        zt(s).start()
        return carry

    lax.fori_loop(3, NZ, send_t, 0)

    w_a(0)

    def stage(fn, s):
        pl.when((s >= 0) & (s < NZ))(lambda: fn(s))

    def w_loop(i, carry):
        stage(w_a, i)
        stage(w_b, i - 1)
        stage(w_c, i - 2)
        stage(w_d, i - 3)
        return carry

    lax.fori_loop(1, NZ + 3, w_loop, 0)

    def w_end(s, carry):
        cw(s).wait_recv()
        return carry

    lax.fori_loop(0, NZ, w_end, 0)
    outs = (gate_out, up_out, down_out)
    saves = [
        pltpu.make_async_copy(
            w.at[m, xb], outs[m].at[:, :, :, pl.ds(LANE * xb, LANE)], out_sem.at[m, xb]
        )
        for m in range(3)
        for xb in range(NX)
    ]
    for save in saves:
        save.start()

    def t_loop(i, carry):
        stage(t_a, i)
        stage(t_b, i - 1)
        stage(t_c, i - 2)
        stage(t_d, i - 3)
        pl.when((i >= 5))(lambda: t_e(i - 4))
        pl.when(i == 4)(lambda: keep())
        return carry

    def keep():
        back[z] = total(0)

    lax.fori_loop(1, NZ + 4, t_loop, 0)

    def finish(s, carry):
        zb(s).wait_recv()
        zb(s).wait_send()
        zt(s).wait_send()
        zw(s).wait_send()
        return carry

    lax.fori_loop(1, NZ, finish, 0)

    def drain(s, carry):
        for j in range(4):
            ag(s, j).wait_send()
            xw(s, j).wait_send()
            rs(s, j).wait_send()
        for k in (1, 2, 3):
            yw(s, k).wait_send()
        cw(s).wait_send()
        return carry

    lax.fori_loop(0, NZ, drain, 0)
    pair.wait_send()
    for save in saves:
        save.wait()
    done = pltpu.make_async_copy(back, back_out, back_sem)
    done.start()
    done.wait()


def exchange(outgoing, pieces):
    any_spec = pl.BlockSpec(memory_space=pl.ANY)
    vmem = pl.BlockSpec(memory_space=pltpu.VMEM)
    ready = jax.ShapeDtypeStruct((32, 2, 32, 512), BF)
    dma = pltpu.SemaphoreType.DMA
    scratch = [
        pltpu.VMEM((NZ, NY, ROWS, WIDE), BF),
        pltpu.VMEM((NZ, NY, ROWS, D), BF),
        pltpu.VMEM((NZ, 2, HALF, D), BF),
        pltpu.VMEM((NZ, 2, ROWS, D), BF),
        pltpu.VMEM((NZ, ROWS, D), BF),
        pltpu.VMEM((NZ, ROWS, D), BF),
        pltpu.VMEM((3, NX, 32, 2, 32, LANE), BF),
        pltpu.VMEM((32, 3, 32, LANE), BF),
        pltpu.VMEM((NZ, FINE, 3, 32, LANE), BF),
        pltpu.VMEM((32, 3, 32, 64), BF),
        dma((NZ,)), dma((NZ,)),
        dma((NZ,)), dma((NZ,)),
        dma((NZ, 4)), dma((NZ, 4)),
        dma((NZ, 3)), dma((NZ, 3)),
        dma((NZ, 4)), dma((NZ, 4)),
        dma((NZ,)), dma((NZ,)),
        dma, dma,
        dma((NZ, 4)), dma((NZ, 4)),
        dma((NZ,)), dma((NZ,)),
        dma((3, NX)), dma,
    ]
    return pl.pallas_call(
        kernel,
        out_shape=(jax.ShapeDtypeStruct((NZ, ROWS, D), BF), ready, ready, ready),
        in_specs=[vmem, vmem],
        out_specs=(any_spec,) * 4,
        scratch_shapes=scratch,
        compiler_params=pltpu.CompilerParams(
            collective_id=0, has_side_effects=True, vmem_limit_bytes=56 * 1024 * 1024
        ),
    )(outgoing, pieces)


def local(
    tokens, expert_group, expert_fine, route_weight, norm_gain, gate_master, up_master, down_master
):
    def piece(m):
        return m.astype(BF).reshape(32, 2, 1, 32, 64)

    gain = norm_gain[None, :, None]
    pieces = jnp.concatenate(
        (piece(gain * gate_master), piece(gain * up_master), piece(down_master)), axis=2
    )
    rows, width = tokens.shape
    per_group = rows // NZ
    widened = tokens.astype(F32)
    normed = (
        widened * lax.rsqrt(jnp.mean(widened * widened, axis=-1, keepdims=True) + EPS)
    ).astype(BF)
    same = (expert_group[:, None] == jnp.arange(NZ)[None, :]).astype(BF)
    ahead = jnp.arange(rows)[:, None] > jnp.arange(rows)[None, :]
    before = jnp.dot(ahead.astype(BF), same, preferred_element_type=F32)
    position = jnp.sum(before * same.astype(F32), axis=1).astype(jnp.int32)
    slot = expert_group * per_group + position
    placing = (jnp.arange(rows, dtype=jnp.int32)[:, None] == slot[None, :]).astype(BF)
    fine_weight = jnp.sum(
        jnp.where(
            expert_fine[:, :, None] == jnp.arange(FINE)[None, None, :],
            route_weight[:, :, None],
            0.0,
        ),
        axis=1,
    )
    high = lax.reduce_precision(fine_weight, 8, 7)
    low = (fine_weight - high).astype(BF)
    packed = jnp.concatenate(
        (normed, high.astype(BF), low, jnp.zeros((rows, LANE - 2 * FINE), BF)), axis=1
    )
    outgoing = jnp.dot(placing, packed, preferred_element_type=F32).astype(BF)
    back, gate, up, down = exchange(outgoing.reshape(NZ, per_group, WIDE), pieces)
    mixed = lax.dot_general(
        placing, back.reshape(rows, width), (((0,), (0,)), ((), ())), preferred_element_type=F32
    ).astype(BF)
    return (mixed,) + tuple(r.reshape(1, D, 512) for r in (gate, up, down))


def solution(mesh):
    fine = Mesh(mesh.devices.reshape(NZ, NY, NX, 2), ("z", "y", "x", "c"))
    fs, tp = ("z", "y"), ("x", "c")
    token = fs + tp
    in_specs = (
        P(token, None),
        P(token),
        P(token, None),
        P(token, None),
        P(fs),
        P(None, fs, tp),
        P(None, fs, tp),
        P(None, fs, tp),
    )
    out_specs = (
        P(token, None),
        P(fs, None, None),
        P(fs, None, None),
        P(fs, None, None),
    )
    return jax.shard_map(local, mesh=fine, in_specs=in_specs, out_specs=out_specs, check_vma=False)
```

time: 307 us -> 160 us (0.52)
  waiting for transfers between devices: 177 us -> 0 us
  Pallas kernels: 0 us -> 140 us
  blocking collectives: 69.6 us -> 0 us
  between operations: 14 us -> 0.74 us
  matrix products: 18.3 us -> 5.26 us
  local copies, waits for them, and re-layouts: 15.1 us -> 7.7 us
  starting transfers between devices: 6.94 us -> 0 us
    pallas_call x0 -> x1, Pallas kernels: none -> 140 us  [exchange(): pl.pallas_call(kernel, out_shape=(jax.ShapeDtypeStruct((NZ, ROWS, D), BF)...]
    all_gather x4 -> x0, waiting for transfers between devices: 107 us -> none  [the longest x3 83.1 us: exchange_weights(): lax.all_gather(a, ('x', 'c'), axis=2, tiled=True)]
    all_to_all x2 -> x0, blocking collectives: 69.6 us -> none  [the longest x1 38.2 us: local(): lax.all_to_all(outgoing, 'z', split_axis=0, concat_axis=0, tiled=True)]
    reduce_scatter x1 -> x0, waiting for transfers between devices: 49.5 us -> none  [local(): summed = lax.psum_scatter(out, 'y', scatter_dimension=0, tiled=True)]
    all_to_all x1 -> x0, waiting for transfers between devices: 20.1 us -> none  [local(): lax.all_to_all(summed.reshape(groups, per_group, width), 'z', split_axis=...]
    dot_general x4 -> x2, matrix products: 16.8 us -> 2.42 us  [the longest x1 1.47 us: local(): outgoing = jnp.dot(placing, packed, preferred_element_type=F32).astype(BF)]
    all_to_all x1 -> x0, starting transfers between devices: 6.73 us -> none  [local(): lax.all_to_all(summed.reshape(groups, per_group, width), 'z', split_axis=...]
  transfers between devices with their start and end apart: 6 -> 0, of which waited for: 6 -> 0; matrix products, arithmetic and copies ran while one was open for 7% -> 0% of each run, Pallas kernels for 0% -> 0%
where the time goes in v2:
time: 160 us
  Pallas kernels  140 us (88%)
  local copies, waits for them, and re-layouts  7.7 us (5%)
  other arithmetic  6.4 us (4%)
  matrix products  5.26 us (3%)
    pallas_call x1, Pallas kernels, exchange(): pl.pallas_call(kernel, out_shape=(jax.ShapeDtypeStruct((NZ, ROWS, D), BF)...  140 us
    unnamed x17, local copies, waits for them, and re-layouts  6.37 us

profile of v2, /device:TPU:1, one launch (start us, length us, event | category | flops | bytes accessed | tf_op | source)
XLA Modules:
  0.0 159.8 jit_solution(14915909693903420132)
XLA Ops:
  0.6 0.0 copy-start
  0.6 1.6 fusion
  2.2 1.0 fusion.2
  3.2 0.7 convert_add_fusion
  3.9 0.7 select_reduce_fusion
  4.6 0.1 copy.15
  4.8 0.1 copy.14
  4.9 1.3 convert_element_type.48
  6.2 0.0 copy-done
  6.2 0.2 fusion.1
  6.5 0.0 copy-start.6
  6.5 1.0 concatenate.6
  7.5 0.0 copy-start.4
  7.6 0.0 copy-start.5
  7.6 1.5 convolution_convert_fusion
  9.0 0.0 copy-done.6
  9.0 0.0 copy-done.4
  9.0 0.3 copy-done.5
  9.4 0.3 multiply_convert_fusion.1
  9.7 1.5 pad_maximum_fusion.pieces
  11.2 139.7 %shard_map.111 = (bf16[8,32,2048]{2,1,0:T(8,128)(2,1)}, bf16[32,2,32,512]{3,2,1,0:T(8,128)(2,1)}, bf16[32,2,32,512]{3,2,1,0:T(8,128)(2,1)}, bf16[32,2,32,512]{3,2,1,0:T(8,128)(2,1)}) custom-call(bf16[8,32,2176]{2,1,0:T(8,128)(2,1)} %bitcast.10, bf16[32,2,3,32,64]{4,3,2,1,0:T(8,128)(2,1)} %pad_maximum_fusion.pieces), custom_call_target="tpu_custom_call" | custom-call | tf_op jit(solution)/shard_map/pallas_call | solution.py:333
  150.9 0.0 copy-start.3
  150.9 2.8 %convolution_convert_fusion.1 = bf16[256,2048]{1,0:T(8,128)(2,1)} fusion(bf16[256,2048]{1,0:T(8,128)(2,1)} %bitcast.17, s32[256]{0:T(256)S(1)} %convert_add_fusion), kind=kOutput, calls=%fused_computation.3 | convolution fusion | flops 269025280 | bytes 2098176 | tf_op jit(solution)/shard_map/dot_general | solution.py:382
  153.7 0.0 copy-done.3
  153.7 0.0 copy-start.2
  153.7 1.3 copy.19
  155.1 1.0 copy-done.2
  156.1 0.0 copy-start.1
  156.1 1.3 copy.20
  157.4 1.0 copy-done.1
  158.4 1.3 copy.21
  (3 shorter events, 0.0 us)
Async XLA Ops:
  0.6 5.6 %copy-start = (bf16[256,2048]{1,0:T(8,128)(2,1)S(1)}, bf16[256,2048]{1,0:T(8,128)(2,1)}, u32[]{:S(2)}) copy-start(bf16[256,2048]{1,0:T(8,128)(2,1)} %param.8) | copy-start | bytes 3145732
  6.5 2.5 %copy-start.6 = (f32[64]{0:T(128)S(1)}, f32[64]{0:T(128)}, u32[]{:S(2)}) copy-start(f32[64]{0:T(128)} %param.12) | copy-start | bytes 772
  7.5 1.5 copy-start.4
  7.6 1.8 %copy-start.5 = (f32[32,64,64]{2,1,0:T(8,128)S(1)}, f32[32,64,64]{2,1,0:T(8,128)}, u32[]{:S(2)}) copy-start(f32[32,64,64]{2,1,0:T(8,128)} %param.14) | copy-start | bytes 1572868
  150.9 2.8 %copy-start.3 = (bf16[32,2,32,512]{3,2,1,0:T(8,128)(2,1)S(1)}, bf16[32,2,32,512]{3,2,1,0:T(8,128)(2,1)}, u32[]{:S(2)}) copy-start(bf16[32,2,32,512]{3,2,1,0:T(8,128)(2,1)} %get-tuple-element.9) | copy-start | bytes 6291460
  153.7 2.3 %copy-start.2 = (bf16[32,2,32,512]{3,2,1,0:T(8,128)(2,1)S(1)}, bf16[32,2,32,512]{3,2,1,0:T(8,128)(2,1)}, u32[]{:S(2)}) copy-start(bf16[32,2,32,512]{3,2,1,0:T(8,128)(2,1)} %get-tuple-element.10) | copy-start | bytes 6291460
  156.1 2.3 %copy-start.1 = (bf16[32,2,32,512]{3,2,1,0:T(8,128)(2,1)S(1)}, bf16[32,2,32,512]{3,2,1,0:T(8,128)(2,1)}, u32[]{:S(2)}) copy-start(bf16[32,2,32,512]{3,2,1,0:T(8,128)(2,1)} %get-tuple-element.11) | copy-start | bytes 6291460

commit v3 on v2

--- a/solution.py
+++ b/solution.py
@@ -24,9 +24,25 @@
     return (odd * far + (1 - odd) * (NZ - far)) % NZ
 
 
+def placing_of(group):
+    count = NZ * ROWS
+    lane = lax.broadcasted_iota(jnp.int32, (count, count), 1)
+    sub = lax.broadcasted_iota(jnp.int32, (count, count), 0)
+    same = lax.broadcasted_iota(jnp.int32, (16, count), 0) == group
+    same = jnp.where(same, 1.0, 0.0)
+    earlier = jnp.where(sub < lane, 1.0, 0.0).astype(BF)
+    before = jnp.dot(same.astype(BF), earlier, preferred_element_type=F32)
+    position = jnp.sum(before * same, axis=0, keepdims=True)
+    slot = group.astype(F32) * ROWS + position
+    return jnp.where(sub.astype(F32) == slot, 1.0, 0.0).astype(BF)
+
+
 def kernel(
-    rows_in, pieces, back_out, gate_out, up_out, down_out,
+    tokens_in, group_in, fine_in, route_in, gain_in, gate_in, up_in, down_in,
+    back_out, gate_out, up_out, down_out,
+    tok, masters, normed, rows_in, pieces,
     a, o, h, f, zsum, back, w, wsend, wz, other,
+    load_sem,
     zt_s, zt_r, zw_s, zw_r, ag_s, ag_r, yw_s, yw_r, xw_s, xw_r, cw_s, cw_r,
     pair_s, pair_r, rs_s, rs_r, zb_s, zb_r, out_sem, back_sem,
 ):
@@ -170,7 +186,8 @@
     def t_c(s):
         ag(s, 2).wait_recv()
         ag(s, 3).wait_recv()
-        expert(s)
+        with jax.named_scope("expert"):
+            expert(s)
         rs(s, 0).start()
         rs(s, 1).start()
 
@@ -189,8 +206,22 @@
 
     def t_e(s):
         zsum[s] = total(s)
-        zb(s).start()
-
+        pl.when(s > 0)(lambda: zb(s).start())
+
+    loads = [
+        pltpu.make_async_copy(src, dst, load_sem.at[k])
+        for k, (src, dst) in enumerate(
+            (
+                (tokens_in, tok),
+                (gate_in, masters.at[0]),
+                (up_in, masters.at[1]),
+                (down_in, masters.at[2]),
+            )
+        )
+    ]
+    for load in loads[1:]:
+        load.start()
+    loads[0].start()
     barrier = pltpu.get_barrier_semaphore()
     peers = (
         [{"z": (z + k) % NZ} for k in range(1, NZ)]
@@ -200,24 +231,78 @@
     )
     for peer in peers:
         pl.semaphore_signal(barrier, inc=1, device_id=peer, device_id_type=MESH)
-    pl.semaphore_wait(barrier, len(peers))
-
-    pair = remote(pieces.at[:, 1 - c], other, pair_s, pair_r, {"c": 1 - c})
+    pair = remote(pieces.at[1 - c], other, pair_s, pair_r, {"c": 1 - c})
+
+    for load in loads[1:]:
+        load.wait()
+    eye = lax.broadcasted_iota(jnp.int32, (64, 64), 0) == lax.broadcasted_iota(
+        jnp.int32, (64, 64), 1
+    )
+    gain = jnp.sum(jnp.where(eye, gain_in[...], 0.0), axis=1, keepdims=True)
+
+    def cast(e, carry):
+        for m in range(3):
+            value = masters[m, e] if m == 2 else gain * masters[m, e]
+            value = value.astype(BF)
+            pieces[0, e, m] = value[:32]
+            pieces[1, e, m] = value[32:]
+        return carry
+
+    with jax.named_scope("cast"):
+        lax.fori_loop(0, NZ * FINE, cast, 0, unroll=4)
+    with jax.named_scope("barrier"):
+        pl.semaphore_wait(barrier, len(peers))
     pair.start()
+
+    loads[0].wait()
+
+    def norm(r, carry):
+        wide = tok[pl.ds(pl.multiple_of(r * ROWS, ROWS), ROWS), :].astype(F32)
+        mean = jnp.sum(wide * wide, axis=1, keepdims=True) * (1.0 / D)
+        normed[pl.ds(pl.multiple_of(r * ROWS, ROWS), ROWS), :] = (
+            wide * lax.rsqrt(mean + EPS)
+        ).astype(BF)
+        return carry
+
+    with jax.named_scope("norm"):
+        lax.fori_loop(0, NZ, norm, 0)
+        count = NZ * ROWS
+        placing = placing_of(group_in[...])
+        entry = lax.broadcasted_iota(jnp.int32, (8, count), 0)
+        fine_id = entry % FINE
+        weight = jnp.where(fine_in[0:1] == fine_id, route_in[0:1], 0.0) + jnp.where(
+            fine_in[1:2] == fine_id, route_in[1:2], 0.0
+        )
+        top = weight.astype(BF).astype(F32)
+        weight = jnp.where(entry < FINE, top, weight - top)
+        weight = jnp.concatenate([weight, jnp.zeros((LANE - 8, count), F32)], axis=0).astype(BF)
+        extra = lax.dot_general(
+            placing, weight, (((1,), (1,)), ((), ())), preferred_element_type=F32
+        )
+        rows_in[:, :, D:WIDE] = extra.astype(BF).reshape(NZ, ROWS, LANE)
+        for nb in range(8):
+            part = jnp.dot(
+                placing, normed[:, 256 * nb : 256 * nb + 256], preferred_element_type=F32
+            )
+            rows_in[:, :, 256 * nb : 256 * nb + 256] = part.astype(BF).reshape(NZ, ROWS, 256)
+
     zt(1).start()
     zt(2).start()
     t_a(0)
-    a[0, 0] = rows_in[z]
-    pair.wait_recv()
+    with jax.named_scope("pair"):
+        pair.wait_recv()
 
     def join(e, carry):
-        mine, theirs = pieces[e, c], other[e]
+        mine, theirs = pieces[c, e], other[e]
         low = jnp.where(c == 0, mine, theirs)
         high = jnp.where(c == 0, theirs, mine)
         wsend[e] = jnp.concatenate([low, high], axis=-1)
         return carry
 
-    lax.fori_loop(0, NZ * FINE, join, 0)
+    with jax.named_scope("join"):
+        lax.fori_loop(0, NZ * FINE, join, 0, unroll=4)
+
+    w_a(0)
 
     def send_w(s, carry):
         zw(s).start()
@@ -230,23 +315,38 @@
         return carry
 
     lax.fori_loop(3, NZ, send_t, 0)
-
-    w_a(0)
+    a[0, 0] = rows_in[z]
+
+    def run(fn, s):
+        with jax.named_scope(fn.__name__):
+            fn(s)
 
     def stage(fn, s):
-        pl.when((s >= 0) & (s < NZ))(lambda: fn(s))
+        pl.when((s >= 0) & (s < NZ))(lambda: run(fn, s))
+
+    def at(i, when, fn, s):
+        pl.when(i == when)(lambda: run(fn, s))
 
     def w_loop(i, carry):
+        stage(w_b, i - 1)
+        at(i, 1, t_a, 1)
         stage(w_a, i)
-        stage(w_b, i - 1)
+        at(i, 2, t_b, 0)
         stage(w_c, i - 2)
+        at(i, 3, t_a, 2)
+        at(i, 4, t_b, 1)
         stage(w_d, i - 3)
+        at(i, 6, t_b, 2)
+        at(i, 8, t_a, 3)
+        at(i, 9, t_a, 4)
+        at(i, 10, t_b, 3)
         return carry
 
     lax.fori_loop(1, NZ + 3, w_loop, 0)
 
     def w_end(s, carry):
-        cw(s).wait_recv()
+        with jax.named_scope("w_end"):
+            cw(s).wait_recv()
         return carry
 
     lax.fori_loop(0, NZ, w_end, 0)
@@ -261,54 +361,108 @@
     for save in saves:
         save.start()
 
+    def slot(i):
+        return (i + 1) % NZ
+
     def t_loop(i, carry):
-        stage(t_a, i)
-        stage(t_b, i - 1)
-        stage(t_c, i - 2)
-        stage(t_d, i - 3)
-        pl.when((i >= 5))(lambda: t_e(i - 4))
-        pl.when(i == 4)(lambda: keep())
-        return carry
-
-    def keep():
-        back[z] = total(0)
-
-    lax.fori_loop(1, NZ + 4, t_loop, 0)
-
-    def finish(s, carry):
-        zb(s).wait_recv()
-        zb(s).wait_send()
-        zt(s).wait_send()
-        zw(s).wait_send()
-        return carry
-
-    lax.fori_loop(1, NZ, finish, 0)
+        pl.when(i < 3)(lambda: run(t_a, i + 5))
+        pl.when(i < 4)(lambda: run(t_b, i + 4))
+        pl.when(i < NZ)(lambda: run(t_c, slot(i)))
+        pl.when((i >= 1) & (i < NZ + 1))(lambda: run(t_d, slot(i - 1)))
+        pl.when(i >= 2)(lambda: run(t_e, slot(i - 2)))
+
+        @pl.when(i < NZ)
+        def _():
+            s = i
+            for j in range(4):
+                xw(s, j).wait_send()
+            for k in (1, 2, 3):
+                yw(s, k).wait_send()
+            cw(s).wait_send()
+
+        @pl.when((i >= 1) & (i < NZ))
+        def _():
+            zw(i).wait_send()
+            zt(i).wait_send()
+
+        return carry
+
+    lax.fori_loop(0, NZ + 2, t_loop, 0)
+    back[z] = zsum[0]
 
     def drain(s, carry):
         for j in range(4):
             ag(s, j).wait_send()
-            xw(s, j).wait_send()
             rs(s, j).wait_send()
-        for k in (1, 2, 3):
-            yw(s, k).wait_send()
-        cw(s).wait_send()
         return carry
 
     lax.fori_loop(0, NZ, drain, 0)
     pair.wait_send()
     for save in saves:
         save.wait()
+
+    def finish(s, carry):
+        with jax.named_scope("finish"):
+            zb(s).wait_recv()
+        zb(s).wait_send()
+        return carry
+
+    lax.fori_loop(1, NZ, finish, 0)
     done = pltpu.make_async_copy(back, back_out, back_sem)
     done.start()
     done.wait()
 
 
-def exchange(outgoing, pieces):
+def settle(back_in, group_in, g_in, u_in, d_in, mixed_out, g_out, u_out, d_out,
+           back, mixed, hold, back_sem, in_sem, out_sem, mixed_sem):
+    first = pltpu.make_async_copy(back_in, back, back_sem)
+    first.start()
+    ins, outs = (g_in, u_in, d_in), (g_out, u_out, d_out)
+    parts = [(m, p) for m in range(3) for p in range(2)]
+    reads = [
+        pltpu.make_async_copy(
+            ins[m].at[pl.ds(D // 2 * p, D // 2)], hold.at[m, p], in_sem.at[m, p]
+        )
+        for m, p in parts
+    ]
+    writes = [
+        pltpu.make_async_copy(
+            hold.at[m, p], outs[m].at[pl.ds(D // 2 * p, D // 2)], out_sem.at[m, p]
+        )
+        for m, p in parts
+    ]
+    for read in reads:
+        read.start()
+    placing = placing_of(group_in[...])
+    first.wait()
+    results = []
+    for nb in range(4):
+        for k in ((0, 1), (2,), (3, 4), (5,))[nb]:
+            reads[k].wait()
+            writes[k].start()
+        cols = pl.ds(512 * nb, 512)
+        mixed[:, cols] = lax.dot_general(
+            placing, back[:, cols], (((0,), (0,)), ((), ())), preferred_element_type=F32
+        ).astype(BF)
+    last = pltpu.make_async_copy(mixed, mixed_out, mixed_sem)
+    last.start()
+    for write in writes:
+        write.wait()
+    last.wait()
+
+
+def exchange(tokens, group, fine, route, gain, gate, up, down):
     any_spec = pl.BlockSpec(memory_space=pl.ANY)
     vmem = pl.BlockSpec(memory_space=pltpu.VMEM)
     ready = jax.ShapeDtypeStruct((32, 2, 32, 512), BF)
     dma = pltpu.SemaphoreType.DMA
+    count = NZ * ROWS
     scratch = [
+        pltpu.VMEM((count, D), BF),
+        pltpu.VMEM((3, 32, 64, 64), F32),
+        pltpu.VMEM((count, D), BF),
+        pltpu.VMEM((NZ, ROWS, WIDE), BF),
+        pltpu.VMEM((2, 32, 3, 32, 64), BF),
         pltpu.VMEM((NZ, NY, ROWS, WIDE), BF),
         pltpu.VMEM((NZ, NY, ROWS, D), BF),
         pltpu.VMEM((NZ, 2, HALF, D), BF),
@@ -319,6 +473,7 @@
         pltpu.VMEM((32, 3, 32, LANE), BF),
         pltpu.VMEM((NZ, FINE, 3, 32, LANE), BF),
         pltpu.VMEM((32, 3, 32, 64), BF),
+        dma((4,)),
         dma((NZ,)), dma((NZ,)),
         dma((NZ,)), dma((NZ,)),
         dma((NZ, 4)), dma((NZ, 4)),
@@ -330,58 +485,46 @@
         dma((NZ,)), dma((NZ,)),
         dma((3, NX)), dma,
     ]
-    return pl.pallas_call(
+    back, *ready = pl.pallas_call(
         kernel,
         out_shape=(jax.ShapeDtypeStruct((NZ, ROWS, D), BF), ready, ready, ready),
-        in_specs=[vmem, vmem],
+        in_specs=[any_spec, vmem, vmem, vmem, vmem, any_spec, any_spec, any_spec],
         out_specs=(any_spec,) * 4,
         scratch_shapes=scratch,
         compiler_params=pltpu.CompilerParams(
             collective_id=0, has_side_effects=True, vmem_limit_bytes=56 * 1024 * 1024
         ),
-    )(outgoing, pieces)
+    )(tokens, group, fine, route, gain, gate, up, down)
+    mixed = jax.ShapeDtypeStruct((count, D), BF)
+    flat = jax.ShapeDtypeStruct((D, 512), BF)
+    return pl.pallas_call(
+        settle,
+        out_shape=(mixed, flat, flat, flat),
+        in_specs=[any_spec, vmem, any_spec, any_spec, any_spec],
+        out_specs=(any_spec,) * 4,
+        scratch_shapes=[
+            pltpu.VMEM((count, D), BF),
+            pltpu.VMEM((count, D), BF),
+            pltpu.VMEM((3, 2, D // 2, 512), BF),
+            dma, dma((3, 2)), dma((3, 2)), dma,
+        ],
+        compiler_params=pltpu.CompilerParams(vmem_limit_bytes=56 * 1024 * 1024),
+    )(back.reshape(count, D), group, *(r.reshape(D, 512) for r in ready))
 
 
 def local(
     tokens, expert_group, expert_fine, route_weight, norm_gain, gate_master, up_master, down_master
 ):
-    def piece(m):
-        return m.astype(BF).reshape(32, 2, 1, 32, 64)
-
-    gain = norm_gain[None, :, None]
-    pieces = jnp.concatenate(
-        (piece(gain * gate_master), piece(gain * up_master), piece(down_master)), axis=2
+    mixed, gate, up, down = exchange(
+        tokens,
+        expert_group.reshape(1, -1),
+        expert_fine.T,
+        route_weight.T,
+        norm_gain.reshape(1, -1),
+        gate_master,
+        up_master,
+        down_master,
     )
-    rows, width = tokens.shape
-    per_group = rows // NZ
-    widened = tokens.astype(F32)
-    normed = (
-        widened * lax.rsqrt(jnp.mean(widened * widened, axis=-1, keepdims=True) + EPS)
-    ).astype(BF)
-    same = (expert_group[:, None] == jnp.arange(NZ)[None, :]).astype(BF)
-    ahead = jnp.arange(rows)[:, None] > jnp.arange(rows)[None, :]
-    before = jnp.dot(ahead.astype(BF), same, preferred_element_type=F32)
-    position = jnp.sum(before * same.astype(F32), axis=1).astype(jnp.int32)
-    slot = expert_group * per_group + position
-    placing = (jnp.arange(rows, dtype=jnp.int32)[:, None] == slot[None, :]).astype(BF)
-    fine_weight = jnp.sum(
-        jnp.where(
-            expert_fine[:, :, None] == jnp.arange(FINE)[None, None, :],
-            route_weight[:, :, None],
-            0.0,
-        ),
-        axis=1,
-    )
-    high = lax.reduce_precision(fine_weight, 8, 7)
-    low = (fine_weight - high).astype(BF)
-    packed = jnp.concatenate(
-        (normed, high.astype(BF), low, jnp.zeros((rows, LANE - 2 * FINE), BF)), axis=1
-    )
-    outgoing = jnp.dot(placing, packed, preferred_element_type=F32).astype(BF)
-    back, gate, up, down = exchange(outgoing.reshape(NZ, per_group, WIDE), pieces)
-    mixed = lax.dot_general(
-        placing, back.reshape(rows, width), (((0,), (0,)), ((), ())), preferred_element_type=F32
-    ).astype(BF)
     return (mixed,) + tuple(r.reshape(1, D, 512) for r in (gate, up, down))
 
 

time: 160 us -> 132 us (0.82)
  Pallas kernels: 140 us -> 131 us
  local copies, waits for them, and re-layouts: 7.7 us -> 0 us
  other arithmetic: 6.4 us -> 0 us
  matrix products: 5.26 us -> 0 us
    pallas_call x1, Pallas kernels: 140 us -> 124 us  [exchange(): pl.pallas_call(kernel, out_shape=(jax.ShapeDtypeStruct((NZ, ROWS, D), BF)...]
    pallas_call x0 -> x1, Pallas kernels: none -> 6.59 us  [exchange(): pl.pallas_call(settle, out_shape=(mixed, flat, flat, flat), in_specs=[any...]
    unnamed x17 -> x0, local copies, waits for them, and re-layouts: 6.37 us -> none
    dot_general x3 -> x0, matrix products: 5.26 us -> none  [the longest x1 2.83 us: local(): lax.dot_general(placing, back.reshape(rows, width), (((0,), (0,)), ((), (...]
    reduce_sum x2 -> x0, other arithmetic: 2.31 us -> none  [the longest x1 1.6 us: local(): jnp.mean(widened * widened, axis=-1, keepdims=True) + EPS]
    convert_element_type x4 -> x0, other arithmetic: 1.88 us -> none  [the longest x2 1.63 us: piece(): return m.astype(BF).reshape(32, 2, 1, 32, 64)]
where the time goes in v3:
time: 132 us
  Pallas kernels  131 us (99%)
    pallas_call x1, Pallas kernels, exchange(): pl.pallas_call(kernel, out_shape=(jax.ShapeDtypeStruct((NZ, ROWS, D), BF)...  124 us
    pallas_call x1, Pallas kernels, exchange(): pl.pallas_call(settle, out_shape=(mixed, flat, flat, flat), in_specs=[any...  6.59 us

profile of v3, /device:TPU:1, one launch (start us, length us, event | category | flops | bytes accessed | tf_op | source)
XLA Modules:
  0.0 131.7 jit_solution(3084485797093371636)
XLA Ops:
  0.6 124.4 %shard_map.111 = (bf16[8,32,2048]{2,1,0:T(8,128)(2,1)}, bf16[32,2,32,512]{3,2,1,0:T(8,128)(2,1)}, bf16[32,2,32,512]{3,2,1,0:T(8,128)(2,1)}, bf16[32,2,32,512]{3,2,1,0:T(8,128)(2,1)}) custom-call(bf16[256,2048]{1,0:T(8,128)(2,1)} %tokens_in.1, s32[1,256]{1,0:T(1,128)} %bitcast.15, s32[2,256]{1,0:T(2,128)} %bitcast.17, f32[2,256]{1,0:T(2,128)} %bitcast.18, ...), custom_call_target="tpu_custom_call" | custom-call | tf_op jit(solution)/shard_map/pallas_call | solution.py:488
  125.1 6.6 %shard_map.112 = (bf16[256,2048]{1,0:T(8,128)(2,1)}, bf16[2048,512]{1,0:T(8,128)(2,1)}, bf16[2048,512]{1,0:T(8,128)(2,1)}, bf16[2048,512]{1,0:T(8,128)(2,1)}) custom-call(bf16[256,2048]{1,0:T(8,128)(2,1)} %bitcast.14, s32[1,256]{1,0:T(1,128)} %bitcast.16, bf16[2048,512]{1,0:T(8,128)(2,1)} %bitcast.11, bf16[2048,512]{1,0:T(8,128)(2,1)} %bitcast.12, ...), custom_call_target="tpu_custom_call" | custom-call | tf_op jit(solution)/shard_map/pallas_call | solution.py:500

commit v4 on v3

--- a/solution.py
+++ b/solution.py
@@ -14,7 +14,6 @@
 HALF = 16
 D = 2048
 LANE = 128
-WIDE = D + LANE
 MESH = pl.DeviceIdType.MESH
 
 
@@ -22,6 +21,11 @@
     far = (s + 1) // 2
     odd = s % 2
     return (odd * far + (1 - odd) * (NZ - far)) % NZ
+
+
+def token_offset_of(k):
+    late = (k + 3) // 8
+    return (NZ + 4 * late + (2 * (k % 2) - 1) * ((k + 1 - 5 * late) // 2)) % NZ
 
 
 def placing_of(group):
@@ -39,12 +43,12 @@
 
 def kernel(
     tokens_in, group_in, fine_in, route_in, gain_in, gate_in, up_in, down_in,
-    back_out, gate_out, up_out, down_out,
-    tok, masters, normed, rows_in, pieces,
-    a, o, h, f, zsum, back, w, wsend, wz, other,
-    load_sem,
-    zt_s, zt_r, zw_s, zw_r, ag_s, ag_r, yw_s, yw_r, xw_s, xw_r, cw_s, cw_r,
-    pair_s, pair_r, rs_s, rs_r, zb_s, zb_r, out_sem, back_sem,
+    back, w,
+    tok, masters, normed, rows_in, pieces, scales, near,
+    a, o, h, f, zsum, wsend, other,
+    load_sem, wt_s, wt_r,
+    zt_s, zt_r, ws_s, ws_r, ag_s, ag_r, xw_s, xw_r, cw_s, cw_r,
+    pair_s, pair_r, rs_s, rs_r, zb_s, zb_r,
 ):
     z, y, x, c = (lax.axis_index(n) for n in ("z", "y", "x", "c"))
     yp, ym = (y + 1) % NY, (y + NY - 1) % NY
@@ -62,12 +66,28 @@
     def from_z(s):
         return (z + NZ - offset_of(s)) % NZ
 
-    def zt(s):
-        return remote(rows_in.at[to_z(s)], a.at[s, 0], zt_s.at[s], zt_r.at[s], {"z": to_z(s)})
-
-    def zw(s):
+    def token_to_z(k):
+        return (z + token_offset_of(k)) % NZ
+
+    def token_from_z(k):
+        return (z + NZ - token_offset_of(k)) % NZ
+
+    def zt(k):
+        t = token_to_z(k)
+        return remote(rows_in.at[t], a.at[k, 0], zt_s.at[k], zt_r.at[k], {"z": t})
+
+    def ws(s, k):
+        tz, ty = to_z(s), (y + k) % NY
         return remote(
-            wsend.at[pl.ds(FINE * to_z(s), FINE)], wz.at[s], zw_s.at[s], zw_r.at[s], {"z": to_z(s)}
+            wsend.at[FINE * tz + ty], w.at[:, x, NY * z + y, c],
+            ws_s.at[s, k], ws_r.at[s, k], {"z": tz, "y": ty},
+        )
+
+    def wt(k, j):
+        tz, ty = token_to_z(k), (y + j) % NY
+        return remote(
+            scales.at[ty, tz // 4], near.at[k, j], wt_s.at[k, j], wt_r.at[k, j],
+            {"z": tz, "y": ty},
         )
 
     def ag(s, j):
@@ -83,12 +103,6 @@
             src, dst, where = a.at[s, 3, pl.ds(HALF, HALF)], a.at[s, 2, pl.ds(HALF, HALF)], ym
         return remote(src, dst, ag_s.at[s, j], ag_r.at[s, j], {"y": where})
 
-    def yw(s, k):
-        t = (y + k) % NY
-        src = wsend.at[FINE * z + t] if isinstance(s, int) and s == 0 else wz.at[s, t]
-        dst = w.at[:, x, NY * from_z(s) + y, c]
-        return remote(src, dst, yw_s.at[s, k - 1], yw_r.at[s, k - 1], {"y": t})
-
     def xw(s, j):
         base = NY * from_z(s)
         if j == 0:
@@ -117,21 +131,12 @@
         return remote(src, dst, rs_s.at[s, j], rs_r.at[s, j], {"y": where})
 
     def zb(s):
-        return remote(zsum.at[s], back.at[z], zb_s.at[s], zb_r.at[s], {"z": from_z(s)})
-
-    def w_a(s):
-        if isinstance(s, int) and s == 0:
-            mine = wsend[FINE * z + y]
-        else:
-            zw(s).wait_recv()
-            mine = wz[s, y]
-        for k in (1, 3, 2):
-            yw(s, k).start()
-        w[:, x, NY * from_z(s) + y, c] = mine
+        return remote(zsum.at[s], back.at[z], zb_s.at[s], zb_r.at[s], {"z": token_from_z(s)})
 
     def w_b(s):
-        for k in (1, 3, 2):
-            yw(s, k).wait_recv()
+        for k in range(1, NY):
+            ws(s, k).wait_recv()
+        pl.when(s > 0)(lambda: ws(s, 0).wait_recv())
         xw(s, 0).start()
         xw(s, 1).start()
 
@@ -159,11 +164,17 @@
         ag(s, 3).start()
 
     def expert(s):
-        data = a[s, :, :, 0:D].reshape(NY * ROWS, D)
-        extra = a[s, :, :, D:WIDE].reshape(NY * ROWS, LANE).astype(F32)
-        lane = lax.broadcasted_iota(jnp.int32, (NY * ROWS, LANE), 1)
-        chosen = (lane == y) | (lane == y + FINE)
-        scale = jnp.sum(jnp.where(chosen, extra, 0.0), axis=1, keepdims=True)
+        data = a[s].reshape(NY * ROWS, D)
+        lane = lax.broadcasted_iota(jnp.int32, (ROWS, LANE), 1)
+        row = lax.broadcasted_iota(jnp.int32, (ROWS, LANE), 0)
+        mine = lane == row + ROWS * (z % 4)
+        scale = jnp.concatenate(
+            [
+                jnp.sum(jnp.where(mine, near[s, j], 0.0), axis=1, keepdims=True)
+                for j in range(NY)
+            ],
+            axis=0,
+        )
         acts = []
         for xb in range(NX):
             both = jnp.concatenate(
@@ -184,6 +195,9 @@
             o[s, :, :, 256 * nb : 256 * nb + 256] = r.reshape(NY, ROWS, 256)
 
     def t_c(s):
+        for j in range(1, NY):
+            wt(s, j).wait_recv()
+        pl.when(s > 0)(lambda: wt(s, 0).wait_recv())
         ag(s, 2).wait_recv()
         ag(s, 3).wait_recv()
         with jax.named_scope("expert"):
@@ -207,6 +221,8 @@
     def t_e(s):
         zsum[s] = total(s)
         pl.when(s > 0)(lambda: zb(s).start())
+        for j in range(4):
+            rs(s, j).wait_send()
 
     loads = [
         pltpu.make_async_copy(src, dst, load_sem.at[k])
@@ -223,14 +239,17 @@
         load.start()
     loads[0].start()
     barrier = pltpu.get_barrier_semaphore()
-    peers = (
-        [{"z": (z + k) % NZ} for k in range(1, NZ)]
-        + [{"y": (y + k) % NY} for k in range(1, NY)]
-        + [{"x": (x + k) % NX} for k in range(1, NX)]
-        + [{"c": 1 - c}]
-    )
+    peers = [{"x": (x + k) % NX} for k in range(1, NX)] + [{"c": 1 - c}]
     for peer in peers:
         pl.semaphore_signal(barrier, inc=1, device_id=peer, device_id_type=MESH)
+
+    def greet(q, carry):
+        peer = {"z": (z + q // NY) % NZ, "y": (y + q % NY) % NY}
+        pl.semaphore_signal(barrier, inc=1, device_id=peer, device_id_type=MESH)
+        return carry
+
+    lax.fori_loop(1, NZ * NY, greet, 0)
+
     pair = remote(pieces.at[1 - c], other, pair_s, pair_r, {"c": 1 - c})
 
     for load in loads[1:]:
@@ -251,7 +270,7 @@
     with jax.named_scope("cast"):
         lax.fori_loop(0, NZ * FINE, cast, 0, unroll=4)
     with jax.named_scope("barrier"):
-        pl.semaphore_wait(barrier, len(peers))
+        pl.semaphore_wait(barrier, NZ * NY - 1 + len(peers))
     pair.start()
 
     loads[0].wait()
@@ -275,20 +294,20 @@
         )
         top = weight.astype(BF).astype(F32)
         weight = jnp.where(entry < FINE, top, weight - top)
-        weight = jnp.concatenate([weight, jnp.zeros((LANE - 8, count), F32)], axis=0).astype(BF)
-        extra = lax.dot_general(
-            placing, weight, (((1,), (1,)), ((), ())), preferred_element_type=F32
-        )
-        rows_in[:, :, D:WIDE] = extra.astype(BF).reshape(NZ, ROWS, LANE)
+        weight = jnp.concatenate([weight, jnp.zeros((8, count), F32)], axis=0).astype(BF)
+        sorted_weight = lax.dot_general(
+            weight, placing, (((1,), (1,)), ((), ())), preferred_element_type=F32
+        )
+        sorted_weight = sorted_weight[0:FINE] + sorted_weight[FINE : 2 * FINE]
+        for e in range(FINE):
+            for p in range(2):
+                scales[e, p] = sorted_weight[e : e + 1, LANE * p : LANE * p + LANE]
         for nb in range(8):
             part = jnp.dot(
                 placing, normed[:, 256 * nb : 256 * nb + 256], preferred_element_type=F32
             )
             rows_in[:, :, 256 * nb : 256 * nb + 256] = part.astype(BF).reshape(NZ, ROWS, 256)
 
-    zt(1).start()
-    zt(2).start()
-    t_a(0)
     with jax.named_scope("pair"):
         pair.wait_recv()
 
@@ -302,47 +321,63 @@
     with jax.named_scope("join"):
         lax.fori_loop(0, NZ * FINE, join, 0, unroll=4)
 
-    w_a(0)
-
-    def send_w(s, carry):
-        zw(s).start()
-        return carry
-
-    lax.fori_loop(1, NZ, send_w, 0)
-
-    def send_t(s, carry):
-        zt(s).start()
-        return carry
-
-    lax.fori_loop(3, NZ, send_t, 0)
+    def send(copy, first, last):
+        def one(s, carry):
+            copy(s)
+            return carry
+
+        lax.fori_loop(first, last, one, 0)
+
+    def send_w(s):
+        for k in (1, 3, 2, 0):
+            ws(s, k).start()
+
+    def send_t(k):
+        zt(k).start()
+        for j in range(NY):
+            wt(k, j).start()
+
+    for k in (1, 3, 2):
+        ws(0, k).start()
+    w[:, x, NY * z + y, c] = wsend[FINE * z + y]
+    send(send_w, 1, 3)
+    send(send_t, 1, 3)
+    t_a(0)
+    send(send_w, 3, NZ)
+    send(send_t, 3, NZ)
+    for j in range(1, NY):
+        wt(0, j).start()
+    near[0, 0] = scales[y, z // 4]
     a[0, 0] = rows_in[z]
 
     def run(fn, s):
         with jax.named_scope(fn.__name__):
             fn(s)
 
-    def stage(fn, s):
-        pl.when((s >= 0) & (s < NZ))(lambda: run(fn, s))
-
-    def at(i, when, fn, s):
-        pl.when(i == when)(lambda: run(fn, s))
+    def at(i, when, *todo):
+        @pl.when(i == when)
+        def _():
+            for fn, s in todo:
+                run(fn, s)
+
+    run(w_b, 0)
+    run(w_b, 1)
+    run(t_a, 1)
 
     def w_loop(i, carry):
-        stage(w_b, i - 1)
-        at(i, 1, t_a, 1)
-        stage(w_a, i)
-        at(i, 2, t_b, 0)
-        stage(w_c, i - 2)
-        at(i, 3, t_a, 2)
-        at(i, 4, t_b, 1)
-        stage(w_d, i - 3)
-        at(i, 6, t_b, 2)
-        at(i, 8, t_a, 3)
-        at(i, 9, t_a, 4)
-        at(i, 10, t_b, 3)
-        return carry
-
-    lax.fori_loop(1, NZ + 3, w_loop, 0)
+        pl.when(i < NZ - 2)(lambda: run(w_b, i + 2))
+        at(i, 0, (t_b, 0))
+        pl.when(i < NZ)(lambda: run(w_c, i))
+        at(i, 0, (t_a, 2))
+        pl.when(i >= 2)(lambda: run(w_d, i - 2))
+        at(i, 2, (t_b, 1))
+        at(i, 4, (t_b, 2))
+        at(i, 5, (t_a, 3), (t_a, 4))
+        at(i, 8, (t_b, 3))
+        at(i, 9, (t_a, 5), (t_b, 4))
+        return carry
+
+    lax.fori_loop(0, NZ + 2, w_loop, 0)
 
     def w_end(s, carry):
         with jax.named_scope("w_end"):
@@ -350,56 +385,41 @@
         return carry
 
     lax.fori_loop(0, NZ, w_end, 0)
-    outs = (gate_out, up_out, down_out)
-    saves = [
-        pltpu.make_async_copy(
-            w.at[m, xb], outs[m].at[:, :, :, pl.ds(LANE * xb, LANE)], out_sem.at[m, xb]
-        )
-        for m in range(3)
-        for xb in range(NX)
-    ]
-    for save in saves:
-        save.start()
-
-    def slot(i):
-        return (i + 1) % NZ
+    order = 0o02765143
 
     def t_loop(i, carry):
-        pl.when(i < 3)(lambda: run(t_a, i + 5))
-        pl.when(i < 4)(lambda: run(t_b, i + 4))
-        pl.when(i < NZ)(lambda: run(t_c, slot(i)))
-        pl.when((i >= 1) & (i < NZ + 1))(lambda: run(t_d, slot(i - 1)))
-        pl.when(i >= 2)(lambda: run(t_e, slot(i - 2)))
+        now, before, last = carry
+        at(i, 4, (t_b, 7))
+        pl.when(i < NZ)(lambda: run(t_c, now % 8))
+        pl.when((i >= 1) & (i < NZ + 1))(lambda: run(t_d, before % 8))
+        at(i, 1, (t_b, 5))
+        at(i, 2, (t_a, 6), (t_a, 7))
+        pl.when(i >= 2)(lambda: run(t_e, last % 8))
+        at(i, 3, (t_b, 6))
 
         @pl.when(i < NZ)
         def _():
             s = i
             for j in range(4):
                 xw(s, j).wait_send()
+                ag(s, j).wait_send()
             for k in (1, 2, 3):
-                yw(s, k).wait_send()
+                ws(s, k).wait_send()
+                wt(s, k).wait_send()
             cw(s).wait_send()
 
         @pl.when((i >= 1) & (i < NZ))
         def _():
-            zw(i).wait_send()
+            ws(i, 0).wait_send()
+            wt(i, 0).wait_send()
             zt(i).wait_send()
 
-        return carry
-
-    lax.fori_loop(0, NZ + 2, t_loop, 0)
+        return now // 8, now, before
+
+    lax.fori_loop(0, NZ + 2, t_loop, (jnp.int32(order), jnp.int32(0), jnp.int32(0)))
     back[z] = zsum[0]
 
-    def drain(s, carry):
-        for j in range(4):
-            ag(s, j).wait_send()
-            rs(s, j).wait_send()
-        return carry
-
-    lax.fori_loop(0, NZ, drain, 0)
     pair.wait_send()
-    for save in saves:
-        save.wait()
 
     def finish(s, carry):
         with jax.named_scope("finish"):
@@ -408,51 +428,34 @@
         return carry
 
     lax.fori_loop(1, NZ, finish, 0)
-    done = pltpu.make_async_copy(back, back_out, back_sem)
-    done.start()
-    done.wait()
-
-
-def settle(back_in, group_in, g_in, u_in, d_in, mixed_out, g_out, u_out, d_out,
-           back, mixed, hold, back_sem, in_sem, out_sem, mixed_sem):
-    first = pltpu.make_async_copy(back_in, back, back_sem)
-    first.start()
-    ins, outs = (g_in, u_in, d_in), (g_out, u_out, d_out)
-    parts = [(m, p) for m in range(3) for p in range(2)]
-    reads = [
-        pltpu.make_async_copy(
-            ins[m].at[pl.ds(D // 2 * p, D // 2)], hold.at[m, p], in_sem.at[m, p]
-        )
-        for m, p in parts
-    ]
+
+def settle(back, w, group_in, mixed_out, g_out, u_out, d_out, mixed, out_sem, mixed_sem):
+    outs = (g_out, u_out, d_out)
     writes = [
         pltpu.make_async_copy(
-            hold.at[m, p], outs[m].at[pl.ds(D // 2 * p, D // 2)], out_sem.at[m, p]
-        )
-        for m, p in parts
+            w.at[m, xb], outs[m].at[:, :, :, pl.ds(LANE * xb, LANE)], out_sem.at[m, xb]
+        )
+        for m in range(3)
+        for xb in range(NX)
     ]
-    for read in reads:
-        read.start()
+    for write in writes:
+        write.start()
     placing = placing_of(group_in[...])
-    first.wait()
-    results = []
+    lasts = []
     for nb in range(4):
-        for k in ((0, 1), (2,), (3, 4), (5,))[nb]:
-            reads[k].wait()
-            writes[k].start()
         cols = pl.ds(512 * nb, 512)
         mixed[:, cols] = lax.dot_general(
             placing, back[:, cols], (((0,), (0,)), ((), ())), preferred_element_type=F32
         ).astype(BF)
-    last = pltpu.make_async_copy(mixed, mixed_out, mixed_sem)
-    last.start()
-    for write in writes:
-        write.wait()
-    last.wait()
+        last = pltpu.make_async_copy(mixed.at[:, cols], mixed_out.at[:, cols], mixed_sem.at[nb])
+        last.start()
+        lasts.append(last)
+    for copy in writes + lasts:
+        copy.wait()
 
 
 def exchange(tokens, group, fine, route, gain, gate, up, down):
-    any_spec = pl.BlockSpec(memory_space=pl.ANY)
+    hbm = pl.BlockSpec(memory_space=pltpu.HBM)
     vmem = pl.BlockSpec(memory_space=pltpu.VMEM)
     ready = jax.ShapeDtypeStruct((32, 2, 32, 512), BF)
     dma = pltpu.SemaphoreType.DMA
@@ -461,55 +464,49 @@
         pltpu.VMEM((count, D), BF),
         pltpu.VMEM((3, 32, 64, 64), F32),
         pltpu.VMEM((count, D), BF),
-        pltpu.VMEM((NZ, ROWS, WIDE), BF),
+        pltpu.VMEM((NZ, ROWS, D), BF),
         pltpu.VMEM((2, 32, 3, 32, 64), BF),
-        pltpu.VMEM((NZ, NY, ROWS, WIDE), BF),
+        pltpu.VMEM((FINE, 2, 1, LANE), F32),
+        pltpu.VMEM((NZ, NY, 1, LANE), F32),
+        pltpu.VMEM((NZ, NY, ROWS, D), BF),
         pltpu.VMEM((NZ, NY, ROWS, D), BF),
         pltpu.VMEM((NZ, 2, HALF, D), BF),
         pltpu.VMEM((NZ, 2, ROWS, D), BF),
         pltpu.VMEM((NZ, ROWS, D), BF),
-        pltpu.VMEM((NZ, ROWS, D), BF),
-        pltpu.VMEM((3, NX, 32, 2, 32, LANE), BF),
         pltpu.VMEM((32, 3, 32, LANE), BF),
-        pltpu.VMEM((NZ, FINE, 3, 32, LANE), BF),
         pltpu.VMEM((32, 3, 32, 64), BF),
         dma((4,)),
-        dma((NZ,)), dma((NZ,)),
+        dma((NZ, 4)), dma((NZ, 4)),
         dma((NZ,)), dma((NZ,)),
         dma((NZ, 4)), dma((NZ, 4)),
-        dma((NZ, 3)), dma((NZ, 3)),
+        dma((NZ, 4)), dma((NZ, 4)),
         dma((NZ, 4)), dma((NZ, 4)),
         dma((NZ,)), dma((NZ,)),
         dma, dma,
         dma((NZ, 4)), dma((NZ, 4)),
         dma((NZ,)), dma((NZ,)),
-        dma((3, NX)), dma,
     ]
-    back, *ready = pl.pallas_call(
+    back, w = pl.pallas_call(
         kernel,
-        out_shape=(jax.ShapeDtypeStruct((NZ, ROWS, D), BF), ready, ready, ready),
-        in_specs=[any_spec, vmem, vmem, vmem, vmem, any_spec, any_spec, any_spec],
-        out_specs=(any_spec,) * 4,
+        out_shape=(
+            pltpu.VMEM((NZ, ROWS, D), BF),
+            pltpu.VMEM((3, NX, 32, 2, 32, LANE), BF),
+        ),
+        in_specs=[hbm, vmem, vmem, vmem, vmem, hbm, hbm, hbm],
+        out_specs=(vmem, vmem),
         scratch_shapes=scratch,
         compiler_params=pltpu.CompilerParams(
             collective_id=0, has_side_effects=True, vmem_limit_bytes=56 * 1024 * 1024
         ),
     )(tokens, group, fine, route, gain, gate, up, down)
-    mixed = jax.ShapeDtypeStruct((count, D), BF)
-    flat = jax.ShapeDtypeStruct((D, 512), BF)
     return pl.pallas_call(
         settle,
-        out_shape=(mixed, flat, flat, flat),
-        in_specs=[any_spec, vmem, any_spec, any_spec, any_spec],
-        out_specs=(any_spec,) * 4,
-        scratch_shapes=[
-            pltpu.VMEM((count, D), BF),
-            pltpu.VMEM((count, D), BF),
-            pltpu.VMEM((3, 2, D // 2, 512), BF),
-            dma, dma((3, 2)), dma((3, 2)), dma,
-        ],
-        compiler_params=pltpu.CompilerParams(vmem_limit_bytes=56 * 1024 * 1024),
-    )(back.reshape(count, D), group, *(r.reshape(D, 512) for r in ready))
+        out_shape=(jax.ShapeDtypeStruct((count, D), BF), ready, ready, ready),
+        in_specs=[vmem, vmem, vmem],
+        out_specs=(hbm,) * 4,
+        scratch_shapes=[pltpu.VMEM((count, D), BF), dma((3, NX)), dma((4,))],
+        compiler_params=pltpu.CompilerParams(vmem_limit_bytes=16 * 1024 * 1024),
+    )(back.reshape(count, D), w, group)
 
 
 def local(

time: 132 us -> 116 us (0.88)
  Pallas kernels: 131 us -> 114 us
    pallas_call x2, Pallas kernels: 131 us -> 114 us  [the longest x1 111 us: exchange(): pl.pallas_call(kernel, out_shape=(pltpu.VMEM((NZ, ROWS, D), BF), pltpu.VM...]
where the time goes in v4:
time: 116 us; the launch traced here: 114 us
  Pallas kernels  114 us (98%)
    pallas_call x1, Pallas kernels, exchange(): pl.pallas_call(kernel, out_shape=(pltpu.VMEM((NZ, ROWS, D), BF), pltpu.VM...  111 us
    pallas_call x1, Pallas kernels, exchange(): pl.pallas_call(settle, out_shape=(jax.ShapeDtypeStruct((count, D), BF), r...  3.18 us

profile of v4, /device:TPU:1, one launch (start us, length us, event | category | flops | bytes accessed | tf_op | source)
XLA Modules:
  0.0 114.4 jit_solution(5286855999794974821)
XLA Ops:
  0.6 0.0 copy-start
  0.6 110.6 %shard_map.111 = (bf16[8,32,2048]{2,1,0:T(8,128)(2,1)S(1)}, bf16[3,4,32,2,32,128]{5,4,3,2,1,0:T(8,128)(2,1)S(1)}) custom-call(bf16[256,2048]{1,0:T(8,128)(2,1)} %tokens_in.1, s32[1,256]{1,0:T(1,128)} %bitcast.9, s32[2,256]{1,0:T(2,128)} %bitcast.11, f32[2,256]{1,0:T(2,128)} %bitcast.12, f32[1,64]{1,0:T(1,128)} %bitcast.13, f32[32,64,64]{2,1,0:T(8,128)} %gate_in.1, ...), custom_call_target="tpu_custom_call" | custom-call | tf_op jit(solution)/shard_map/pallas_call | solution.py:489
  111.2 0.0 copy-done
  111.2 3.2 %shard_map.112 = (bf16[256,2048]{1,0:T(8,128)(2,1)}, bf16[32,2,32,512]{3,2,1,0:T(8,128)(2,1)}, bf16[32,2,32,512]{3,2,1,0:T(8,128)(2,1)}, bf16[32,2,32,512]{3,2,1,0:T(8,128)(2,1)}) custom-call(bf16[256,2048]{1,0:T(8,128)(2,1)S(1)} %bitcast.8, bf16[3,4,32,2,32,128]{5,4,3,2,1,0:T(8,128)(2,1)S(1)} %get-tuple-element.11.w, s32[1,256]{1,0:T(1,128)S(1)} %bitcast.10), custom_call_target="tpu_custom_call" | custom-call | tf_op jit(solution)/shard_map/pallas_call | solution.py:502
Async XLA Ops:
  0.6 110.6 %copy-start = (s32[256]{0:T(256)S(1)}, s32[256]{0:T(256)}, u32[]{:S(2)}) copy-start(s32[256]{0:T(256)} %param.9) | copy-start | bytes 3076

commit v5 on v4

v5 whole, which is shorter than its diff:
```python
import jax
import jax.numpy as jnp
from jax import lax
from jax.experimental import pallas as pl
from jax.experimental.pallas import tpu as pltpu
from jax.sharding import Mesh, PartitionSpec as P

FINE = 4
EPS = 1e-06
BF = jnp.bfloat16
F32 = jnp.float32
NZ, NY, NX = 8, 4, 4
ROWS = 32
HALF = 16
PAIRED = 4
SENT = ("zt", "wt0", "wt", "ws0", "ws", "ag", "pg", "sw", "xw", "xv", "cw", "cv", "rs", "pr", "zb", "pair")
D = 2048
LANE = 128
MESH = pl.DeviceIdType.MESH


def offset_of(s):
    far = (s + 1) // 2
    odd = s % 2
    return (odd * far + (1 - odd) * (NZ - far)) % NZ


def placing_of(group):
    count = NZ * ROWS
    lane = lax.broadcasted_iota(jnp.int32, (count, count), 1)
    sub = lax.broadcasted_iota(jnp.int32, (count, count), 0)
    same = lax.broadcasted_iota(jnp.int32, (16, count), 0) == group
    same = jnp.where(same, 1.0, 0.0)
    earlier = jnp.where(sub < lane, 1.0, 0.0).astype(BF)
    before = jnp.dot(same.astype(BF), earlier, preferred_element_type=F32)
    position = jnp.sum(before * same, axis=0, keepdims=True)
    slot = group.astype(F32) * ROWS + position
    return jnp.where(sub.astype(F32) == slot, 1.0, 0.0).astype(BF)


def kernel(
    tokens_in, group_hbm, fine_hbm, route_hbm, gain_hbm, gate_in, up_in, down_in,
    back, w,
    group_in, fine_in, route_in, gain_in, tok, masters, normed, rows_in, pieces, scales, near,
    a, o, h, f, zsum, wsend, other, w2, acc,
    load_sem, sent, pair_r, cw_r, cv_r, zb_r, zt_r, wt_r, ws_r, sw_r, pg_r, pr_r,
    h_r, f_r, ag_r, xw_r, xv_r,
):
    z, y, x, c = (lax.axis_index(n) for n in ("z", "y", "x", "c"))
    yp, ym = (y + 1) % NY, (y + NY - 1) % NY
    sibling, partner = y + 1 - 2 * (y % 2), NY - 1 - y
    xp, xm = (x + 1) % NX, (x + NX - 1) % NX

    def remote(src, dst, ss, rs, where):
        return pltpu.make_async_remote_copy(
            src_ref=src, dst_ref=dst, send_sem=ss, recv_sem=rs,
            device_id=where, device_id_type=MESH,
        )

    def sem_of(name):
        return sent.at[SENT.index(name)]

    def arrived(ref, sem):
        remote(ref, ref, sem, sem, {"c": 1 - c}).wait_recv()

    def all_sent(ref, name):
        remote(ref, ref, sem_of(name), sem_of(name), {"c": 1 - c}).wait_send()

    def to_z(s):
        return (z + offset_of(s)) % NZ

    def from_z(s):
        return (z + NZ - offset_of(s)) % NZ

    def zt(k):
        t = to_z(k)
        return remote(rows_in.at[t], a.at[k, 0], sem_of("zt"), zt_r.at[k], {"z": t})

    def ws(s, k, name="ws"):
        tz, ty = to_z(s), (y + k) % NY
        return remote(
            wsend.at[FINE * tz + ty], w.at[:, x, NY * z + y, c],
            sem_of(name), ws_r.at[s], {"z": tz, "y": ty},
        )

    def wt(k, j, name="wt"):
        tz, ty = to_z(k), (y + j) % NY
        return remote(
            scales.at[tz // 4, ty // 2], near.at[k, j], sem_of(name), wt_r.at[k],
            {"z": tz, "y": ty},
        )

    def ag(s, j):
        if j == 0:
            src, dst, where = a.at[s, 0], a.at[s, 1], yp
        elif j == 1:
            src, dst, where = a.at[s, 0], a.at[s, 3], ym
        elif j == 2:
            src, dst, where = a.at[s, 1, pl.ds(0, HALF)], a.at[s, 2, pl.ds(0, HALF)], yp
        else:
            src, dst, where = a.at[s, 3, pl.ds(HALF, HALF)], a.at[s, 2, pl.ds(HALF, HALF)], ym
        return remote(src, dst, sem_of("ag"), ag_r.at[s, min(j, 2)], {"y": where})

    def sw(s):
        rows = pl.ds(NY * from_z(s), NY)
        return remote(
            w.at[:, x, rows, c], w2.at[:, x, rows, c], sem_of("sw"), sw_r.at[s], {"y": sibling}
        )

    def gather_x(buf, name, rr, s, j):
        base = NY * from_z(s)
        if j == 0:
            part, where = buf.at[:, x, pl.ds(base, NY), c], xp
        elif j == 1:
            part, where = buf.at[:, x, pl.ds(base, NY), c], xm
        elif j == 2:
            part, where = buf.at[:, xm, pl.ds(base, 2), c], xp
        else:
            part, where = buf.at[:, xp, pl.ds(base + 2, 2), c], xm
        return remote(part, part, sem_of(name), rr.at[s, min(j, 2)], {"x": where})

    def xw(s, j):
        return gather_x(w, "xw", xw_r, s, j)

    def xv(s, j):
        return gather_x(w2, "xv", xv_r, s, j)

    def far_column(buf, s):
        return buf.at[:, (x + 2) % NX, pl.ds(NY * from_z(s), NY), c]

    def cw(s):
        part = w.at[:, :, pl.ds(NY * from_z(s), NY), c]
        return remote(part, part, sem_of("cw"), cw_r, {"c": 1 - c})

    def cv(s):
        part = w2.at[:, :, pl.ds(NY * from_z(s), NY), c]
        return remote(part, part, sem_of("cv"), cv_r, {"c": 1 - c})

    def pg(k):
        src = rows_in.at[z] if isinstance(k, int) and k == 0 else a.at[k, 0]
        return remote(src, a.at[k, 1], sem_of("pg"), pg_r.at[k], {"y": partner})

    def pr(k):
        return remote(o.at[k, 1], f.at[k, 0], sem_of("pr"), pr_r.at[k], {"y": partner})

    def rs(s, j):
        if j == 0:
            src, dst, rr, where = o.at[s, 2, pl.ds(0, HALF)], h.at[s, 0], h_r, ym
        elif j == 1:
            src, dst, rr, where = o.at[s, 2, pl.ds(HALF, HALF)], h.at[s, 1], h_r, yp
        elif j == 2:
            src, dst, rr, where = o.at[s, 1], f.at[s, 0], f_r, ym
        else:
            src, dst, rr, where = o.at[s, 3], f.at[s, 1], f_r, yp
        return remote(src, dst, sem_of("rs"), rr.at[s], {"y": where})

    def zb(s):
        return remote(zsum.at[s], back.at[z], sem_of("zb"), zb_r, {"z": from_z(s)})

    def w_b(s):
        if isinstance(s, int) and s == 0:
            arrived(wsend.at[pl.ds(0, NY - 1)], ws_r.at[s])
        else:
            arrived(wsend.at[pl.ds(0, NY)], ws_r.at[s])
        xw(s, 0).start()
        xw(s, 1).start()
        sw(s).start()

    def w_c(s):
        xw(s, 0).wait_recv()
        xw(s, 2).start()
        xw(s, 1).wait_recv()
        xw(s, 3).start()

    def w_d(s):
        arrived(far_column(w, s), xw_r.at[s, 2])
        cw(s).start()

    def v_b(s):
        sw(s).wait_recv()
        xv(s, 0).start()
        xv(s, 1).start()

    def v_c(s):
        xv(s, 0).wait_recv()
        xv(s, 2).start()
        xv(s, 1).wait_recv()
        xv(s, 3).start()

    def v_d(s):
        arrived(far_column(w2, s), xv_r.at[s, 2])
        cv(s).start()

    def t_a(s):
        zt(s).wait_recv()
        ag(s, 0).start()
        ag(s, 1).start()

    def p_a(k):
        if k > 0:
            zt(k).wait_recv()
        pg(k).start()

    def t_b(s):
        ag(s, 0).wait_recv()
        ag(s, 2).start()
        ag(s, 1).wait_recv()
        ag(s, 3).start()

    def scale_of(s, sources, which):
        lane = lax.broadcasted_iota(jnp.int32, (ROWS, LANE), 1)
        row = lax.broadcasted_iota(jnp.int32, (ROWS, LANE), 0)
        mine = lane == row + ROWS * (z % 4)
        return jnp.concatenate(
            [
                jnp.sum(jnp.where(mine, near[s, j, which], 0.0), axis=1, keepdims=True)
                for j in sources
            ],
            axis=0,
        )

    def expert(s, sources, buf, which, take):
        count = len(sources)
        data = a[s, 0:count].reshape(count * ROWS, D)
        parts = []
        for xb in range(NX):
            both = jnp.concatenate(
                [buf[0, xb].reshape(D, LANE), buf[1, xb].reshape(D, LANE)], axis=1
            )
            r = jnp.dot(data, both, preferred_element_type=F32)
            g, u = r[:, :LANE], r[:, LANE:]
            parts.append((g / (1.0 + jnp.exp(-g)) * u).astype(BF))
        act = jnp.concatenate(parts, axis=1)
        scale = scale_of(s, sources, which)
        for nb in range(8):
            rhs = jnp.concatenate(
                [buf[2, xb, 4 * nb : 4 * nb + 4].reshape(256, LANE) for xb in range(NX)],
                axis=1,
            )
            r = lax.dot_general(act, rhs, (((1,), (1,)), ((), ())), preferred_element_type=F32)
            take(slice(256 * nb, 256 * nb + 256), r.astype(BF).astype(F32) * scale)

    def await_scales(s):
        if isinstance(s, int):
            near_s = near.at[s, pl.ds(1, NY - 1)] if s == 0 else near.at[s]
            arrived(near_s, wt_r.at[s])
        else:
            pl.when(s == 0)(lambda: arrived(near.at[0, pl.ds(1, NY - 1)], wt_r.at[0]))
            pl.when(s > 0)(lambda: arrived(near.at[s], wt_r.at[s]))

    def t_c(s):
        arrived(near.at[s], wt_r.at[s])
        arrived(a.at[s, 2], ag_r.at[s, 2])

        def take(cols, r):
            o[s, :, :, cols] = r.astype(BF).reshape(NY, ROWS, 256)

        expert(s, range(NY), w, y % 2, take)
        rs(s, 0).start()
        rs(s, 1).start()

    pair_sources = (0, 1 + 2 * (y % 2))

    def p_b(k):
        await_scales(k)
        pg(k).wait_recv()

        def take(cols, r):
            acc[k, :, cols] = r

        expert(k, pair_sources, w, y % 2, take)

    def p_c(k):
        def take(cols, r):
            o[k, 0:2, :, cols] = (acc[k, :, cols] + r).astype(BF).reshape(2, ROWS, 256)

        expert(k, pair_sources, w2, 1 - y % 2, take)
        pr(k).start()

    def p_e(k):
        pr(k).wait_recv()
        zsum[k] = (o[k, 0].astype(F32) + f[k, 0].astype(F32)).astype(BF)
        pl.when(k > 0)(lambda: zb(k).start())

    def t_d(s):
        arrived(h.at[s], h_r.at[s])
        o[s, 1, 0:HALF] = (o[s, 1, 0:HALF].astype(F32) + h[s, 0].astype(F32)).astype(BF)
        rs(s, 2).start()
        o[s, 3, HALF:ROWS] = (o[s, 3, HALF:ROWS].astype(F32) + h[s, 1].astype(F32)).astype(BF)
        rs(s, 3).start()

    def t_e(s):
        arrived(f.at[s], f_r.at[s])
        zsum[s] = (
            o[s, 0].astype(F32) + f[s, 0].astype(F32) + f[s, 1].astype(F32)
        ).astype(BF)
        zb(s).start()

    loads = [
        pltpu.make_async_copy(src, dst, load_sem.at[k])
        for k, (src, dst) in enumerate(
            (
                (gain_hbm, gain_in),
                (gate_in, masters.at[0]),
                (up_in, masters.at[1]),
                (down_in, masters.at[2]),
                (tokens_in, tok),
                (group_hbm, group_in),
                (fine_hbm, fine_in),
                (route_hbm, route_in),
            )
        )
    ]
    for load in loads:
        load.start()
    barrier = pltpu.get_barrier_semaphore()
    peers = [{"x": (x + k) % NX} for k in range(1, NX)] + [{"c": 1 - c}]
    for peer in peers:
        pl.semaphore_signal(barrier, inc=1, device_id=peer, device_id_type=MESH)

    def greet(q, carry):
        peer = {"z": (z + q // NY) % NZ, "y": (y + q % NY) % NY}
        pl.semaphore_signal(barrier, inc=1, device_id=peer, device_id_type=MESH)
        return carry

    lax.fori_loop(1, NZ * NY, greet, 0)

    pair = remote(pieces.at[1 - c], other, sem_of("pair"), pair_r, {"c": 1 - c})

    for load in loads[:4]:
        load.wait()
    eye = lax.broadcasted_iota(jnp.int32, (64, 64), 0) == lax.broadcasted_iota(
        jnp.int32, (64, 64), 1
    )
    gain = jnp.sum(jnp.where(eye, gain_in[...], 0.0), axis=1, keepdims=True)

    def cast(e, carry):
        for m in range(3):
            value = masters[m, e] if m == 2 else gain * masters[m, e]
            value = value.astype(BF)
            pieces[0, e, m] = value[:32]
            pieces[1, e, m] = value[32:]
        return carry

    with jax.named_scope("cast"):
        lax.fori_loop(0, NZ * FINE, cast, 0, unroll=4)
    with jax.named_scope("barrier"):
        pl.semaphore_wait(barrier, NZ * NY - 1 + len(peers))
    pair.start()

    for load in loads[4:]:
        load.wait()

    def norm(r, carry):
        wide = tok[pl.ds(pl.multiple_of(r * ROWS, ROWS), ROWS), :].astype(F32)
        mean = jnp.sum(wide * wide, axis=1, keepdims=True) * (1.0 / D)
        normed[pl.ds(pl.multiple_of(r * ROWS, ROWS), ROWS), :] = (
            wide * lax.rsqrt(mean + EPS)
        ).astype(BF)
        return carry

    with jax.named_scope("norm"):
        lax.fori_loop(0, NZ, norm, 0)
        count = NZ * ROWS
        placing = placing_of(group_in[...])
        entry = lax.broadcasted_iota(jnp.int32, (8, count), 0)
        fine_id = entry % FINE
        weight = jnp.where(fine_in[0:1] == fine_id, route_in[0:1], 0.0) + jnp.where(
            fine_in[1:2] == fine_id, route_in[1:2], 0.0
        )
        top = weight.astype(BF).astype(F32)
        weight = jnp.where(entry < FINE, top, weight - top)
        weight = jnp.concatenate([weight, jnp.zeros((8, count), F32)], axis=0).astype(BF)
        sorted_weight = lax.dot_general(
            weight, placing, (((1,), (1,)), ((), ())), preferred_element_type=F32
        )
        sorted_weight = sorted_weight[0:FINE] + sorted_weight[FINE : 2 * FINE]
        for e in range(FINE):
            for p in range(2):
                scales[p, e // 2, e % 2] = sorted_weight[e : e + 1, LANE * p : LANE * p + LANE]
        for nb in range(8):
            part = jnp.dot(
                placing, normed[:, 256 * nb : 256 * nb + 256], preferred_element_type=F32
            )
            rows_in[:, :, 256 * nb : 256 * nb + 256] = part.astype(BF).reshape(NZ, ROWS, 256)

    with jax.named_scope("pair"):
        pair.wait_recv()

    def join(e, carry):
        mine, theirs = pieces[c, e], other[e]
        low = jnp.where(c == 0, mine, theirs)
        high = jnp.where(c == 0, theirs, mine)
        wsend[e] = jnp.concatenate([low, high], axis=-1)
        return carry

    with jax.named_scope("join"):
        lax.fori_loop(0, NZ * FINE, join, 0, unroll=4)

    def send(copy, first, last):
        def one(s, carry):
            copy(s)
            return carry

        lax.fori_loop(first, last, one, 0)

    def send_w(s):
        for k in (1, 3, 2, 0):
            ws(s, k).start()

    def send_t(k):
        zt(k).start()
        for j in range(NY):
            wt(k, j).start()

    for k in (1, 3, 2):
        ws(0, k, "ws0").start()
    w[:, x, NY * z + y, c] = wsend[FINE * z + y]
    send(send_w, 1, 3)
    send(send_t, 1, 3)
    p_a(0)
    send(send_w, 3, NZ)
    send(send_t, 3, NZ)
    for j in range(1, NY):
        wt(0, j, "wt0").start()
    near[0, 0] = scales[z // 4, y // 2]
    a[0, 0] = rows_in[z]

    def run(fn, s):
        with jax.named_scope(fn.__name__):
            fn(s)

    def at(i, when, *todo):
        @pl.when(i == when)
        def _():
            for fn, s in todo:
                run(fn, s)

    run(w_b, 0)
    run(w_b, 1)
    run(p_a, 1)
    run(p_a, 2)

    def w_loop(i, carry):
        pl.when(i < NZ - 2)(lambda: run(w_b, i + 2))
        pl.when(i < NZ)(lambda: run(w_c, i))
        pl.when(i >= 2)(lambda: run(w_d, i - 2))
        at(i, 5, (t_a, 4), (p_a, 3))
        at(i, 6, (v_b, 0))
        at(i, 7, (v_b, 1))
        at(i, 8, (v_b, 2), (t_b, 4))
        at(i, 9, (t_a, 5), (t_a, 6))
        return carry

    lax.fori_loop(0, NZ + 2, w_loop, 0)

    with jax.named_scope("w_end"):
        arrived(w.at[:, :, :, 0], cw_r)
    def v_start(s, carry):
        v_b(s)
        return carry

    def t_loop(i, carry):
        run(t_c, i + PAIRED)

        @pl.when(i == 0)
        def _():
            lax.fori_loop(3, NZ, v_start, 0)

        at(i, 0, (v_c, 0), (v_c, 1))
        run(p_b, (i + 1) % PAIRED)
        at(i, 0, (t_b, 5), (v_c, 2), (t_b, 6), (t_a, 7), (t_d, 4), (v_c, 3))
        at(i, 1, (v_c, 4))
        at(i, 2, (v_c, 5), (t_b, 7), (t_e, 4), (v_c, 6), (t_d, 5), (v_d, 0), (v_d, 1), (t_d, 6))
        at(
            i, 3, (v_c, 7), (v_d, 2), (t_e, 5), (v_d, 3), (v_d, 4), (t_e, 6), (v_d, 5),
            (t_d, 7), (v_d, 6), (v_d, 7),
        )
        return carry

    lax.fori_loop(0, NZ - PAIRED, t_loop, 0)
    with jax.named_scope("v_end"):
        arrived(w2.at[:, :, :, 0], cv_r)

    def p_at(i):
        return i % 3 + 3 * ((3 - i) // 3)

    def p_loop(i, carry):
        run(p_c, p_at(i))
        at(i, 1, (t_e, 7))
        pl.when(i >= 1)(lambda: run(p_e, p_at(i - 1)))
        return carry

    lax.fori_loop(0, PAIRED, p_loop, 0)
    run(p_e, 0)
    back[z] = zsum[0]
    many = NZ - 1
    all_sent(pieces.at[0], "pair")
    all_sent(rows_in.at[pl.ds(0, many)], "zt")
    all_sent(near.at[0, pl.ds(0, NY - 1)], "wt0")
    all_sent(near.at[pl.ds(0, many)], "wt")
    all_sent(wsend.at[pl.ds(0, NY - 1)], "ws0")
    all_sent(wsend.at[pl.ds(0, many * NY)], "ws")
    all_sent(wsend, "sw")
    all_sent(w.at[:, pl.ds(0, 3), :, 0], "xw")
    all_sent(w2.at[:, pl.ds(0, 3), :, 0], "xv")
    all_sent(w.at[:, :, :, 0], "cw")
    all_sent(w2.at[:, :, :, 0], "cv")
    all_sent(a.at[pl.ds(PAIRED, NZ - PAIRED), pl.ds(0, 3)], "ag")
    all_sent(o.at[pl.ds(PAIRED, NZ - PAIRED), pl.ds(0, 3)], "rs")
    all_sent(a.at[pl.ds(0, PAIRED), 0], "pg")
    all_sent(o.at[pl.ds(0, PAIRED), 0], "pr")
    with jax.named_scope("finish"):
        arrived(back.at[pl.ds(0, many)], zb_r)
    all_sent(back.at[pl.ds(0, many)], "zb")


def settle(back, w, group_in, mixed_out, g_out, u_out, d_out, mixed, out_sem, mixed_sem):
    outs = (g_out, u_out, d_out)
    writes = [
        pltpu.make_async_copy(
            w.at[m, xb], outs[m].at[:, :, :, pl.ds(LANE * xb, LANE)], out_sem.at[m, xb]
        )
        for m in range(3)
        for xb in range(NX)
    ]
    for write in writes:
        write.start()
    placing = placing_of(group_in[...])
    lasts = []
    for nb in range(4):
        cols = pl.ds(512 * nb, 512)
        mixed[:, cols] = lax.dot_general(
            placing, back[:, cols], (((0,), (0,)), ((), ())), preferred_element_type=F32
        ).astype(BF)
        last = pltpu.make_async_copy(mixed.at[:, cols], mixed_out.at[:, cols], mixed_sem.at[nb])
        last.start()
        lasts.append(last)
    for copy in writes + lasts:
        copy.wait()


def exchange(tokens, group, fine, route, gain, gate, up, down):
    hbm = pl.BlockSpec(memory_space=pltpu.HBM)
    vmem = pl.BlockSpec(memory_space=pltpu.VMEM)
    ready = jax.ShapeDtypeStruct((32, 2, 32, 512), BF)
    dma = pltpu.SemaphoreType.DMA
    count = NZ * ROWS
    scratch = [
        pltpu.VMEM((1, count), jnp.int32),
        pltpu.VMEM((2, count), jnp.int32),
        pltpu.VMEM((2, count), F32),
        pltpu.VMEM((1, 64), F32),
        pltpu.VMEM((count, D), BF),
        pltpu.VMEM((3, 32, 64, 64), F32),
        pltpu.VMEM((count, D), BF),
        pltpu.VMEM((NZ, ROWS, D), BF),
        pltpu.VMEM((2, 32, 3, 32, 64), BF),
        pltpu.VMEM((2, 2, 2, 1, LANE), F32),
        pltpu.VMEM((NZ, NY, 2, 1, LANE), F32),
        pltpu.VMEM((NZ, NY, ROWS, D), BF),
        pltpu.VMEM((NZ, NY, ROWS, D), BF),
        pltpu.VMEM((NZ, 2, HALF, D), BF),
        pltpu.VMEM((NZ, 2, ROWS, D), BF),
        pltpu.VMEM((NZ, ROWS, D), BF),
        pltpu.VMEM((32, 3, 32, LANE), BF),
        pltpu.VMEM((32, 3, 32, 64), BF),
        pltpu.VMEM((3, NX, 32, 2, 32, LANE), BF),
        pltpu.VMEM((PAIRED, 2 * ROWS, D), F32),
        dma((8,)), dma((len(SENT),)),
        dma, dma, dma, dma,
        dma((NZ,)), dma((NZ,)), dma((NZ,)), dma((NZ,)),
        dma((PAIRED,)), dma((PAIRED,)),
        dma((NZ,)), dma((NZ,)),
        dma((NZ, 3)), dma((NZ, 3)), dma((NZ, 3)),
    ]
    back, w = pl.pallas_call(
        kernel,
        out_shape=(
            pltpu.VMEM((NZ, ROWS, D), BF),
            pltpu.VMEM((3, NX, 32, 2, 32, LANE), BF),
        ),
        in_specs=[hbm] * 8,
        out_specs=(vmem, vmem),
        scratch_shapes=scratch,
        compiler_params=pltpu.CompilerParams(
            collective_id=0, has_side_effects=True, vmem_limit_bytes=56 * 1024 * 1024
        ),
    )(tokens, group, fine, route, gain, gate, up, down)
    return pl.pallas_call(
        settle,
        out_shape=(jax.ShapeDtypeStruct((count, D), BF), ready, ready, ready),
        in_specs=[vmem, vmem, vmem],
        out_specs=(hbm,) * 4,
        scratch_shapes=[pltpu.VMEM((count, D), BF), dma((3, NX)), dma((4,))],
        compiler_params=pltpu.CompilerParams(vmem_limit_bytes=16 * 1024 * 1024),
    )(back.reshape(count, D), w, group)


def local(
    tokens, expert_group, expert_fine, route_weight, norm_gain, gate_master, up_master, down_master
):
    mixed, gate, up, down = exchange(
        tokens,
        expert_group.reshape(1, -1),
        expert_fine.T,
        route_weight.T,
        norm_gain.reshape(1, -1),
        gate_master,
        up_master,
        down_master,
    )
    return (mixed,) + tuple(r.reshape(1, D, 512) for r in (gate, up, down))


def solution(mesh):
    fine = Mesh(mesh.devices.reshape(NZ, NY, NX, 2), ("z", "y", "x", "c"))
    fs, tp = ("z", "y"), ("x", "c")
    token = fs + tp
    in_specs = (
        P(token, None),
        P(token),
        P(token, None),
        P(token, None),
        P(fs),
        P(None, fs, tp),
        P(None, fs, tp),
        P(None, fs, tp),
    )
    out_specs = (
        P(token, None),
        P(fs, None, None),
        P(fs, None, None),
        P(fs, None, None),
    )
    return jax.shard_map(local, mesh=fine, in_specs=in_specs, out_specs=out_specs, check_vma=False)
```

time: 116 us -> 107 us (0.922); the launches traced: 114 us -> 107 us
  Pallas kernels: 114 us -> 106 us
    pallas_call x1, Pallas kernels: 111 us -> 103 us  [exchange(): pl.pallas_call(kernel, out_shape=(pltpu.VMEM((NZ, ROWS, D), BF), pltpu.VM...]
where the time goes in v5:
time: 107 us
  Pallas kernels  106 us (99%)
    pallas_call x1, Pallas kernels, exchange(): pl.pallas_call(kernel, out_shape=(pltpu.VMEM((NZ, ROWS, D), BF), pltpu.VM...  103 us
    pallas_call x1, Pallas kernels, exchange(): pl.pallas_call(settle, out_shape=(jax.ShapeDtypeStruct((count, D), BF), r...  3.18 us

profile of v5, /device:TPU:1, one launch (start us, length us, event | category | flops | bytes accessed | tf_op | source)
XLA Modules:
  0.0 106.8 jit_solution(2512595263398632810)
XLA Ops:
  0.6 0.0 copy-start
  0.6 103.0 %shard_map.111 = (bf16[8,32,2048]{2,1,0:T(8,128)(2,1)S(1)}, bf16[3,4,32,2,32,128]{5,4,3,2,1,0:T(8,128)(2,1)S(1)}) custom-call(bf16[256,2048]{1,0:T(8,128)(2,1)} %tokens_in.1, s32[1,256]{1,0:T(1,128)} %bitcast.9, s32[2,256]{1,0:T(2,128)} %bitcast.11, f32[2,256]{1,0:T(2,128)} %bitcast.12, f32[1,64]{1,0:T(1,128)} %bitcast.13, f32[32,64,64]{2,1,0:T(8,128)} %gate_in.1, ...), custom_call_target="tpu_custom_call" | custom-call | tf_op jit(solution)/shard_map/pallas_call | solution.py:577
  103.6 0.0 copy-done
  103.6 3.2 %shard_map.112 = (bf16[256,2048]{1,0:T(8,128)(2,1)}, bf16[32,2,32,512]{3,2,1,0:T(8,128)(2,1)}, bf16[32,2,32,512]{3,2,1,0:T(8,128)(2,1)}, bf16[32,2,32,512]{3,2,1,0:T(8,128)(2,1)}) custom-call(bf16[256,2048]{1,0:T(8,128)(2,1)S(1)} %bitcast.8, bf16[3,4,32,2,32,128]{5,4,3,2,1,0:T(8,128)(2,1)S(1)} %get-tuple-element.11.w, s32[1,256]{1,0:T(1,128)S(1)} %bitcast.10), custom_call_target="tpu_custom_call" | custom-call | tf_op jit(solution)/shard_map/pallas_call | solution.py:590
Async XLA Ops:
  0.6 103.0 %copy-start = (s32[256]{0:T(256)S(1)}, s32[256]{0:T(256)}, u32[]{:S(2)}) copy-start(s32[256]{0:T(256)} %param.9) | copy-start | bytes 3076

commit v6 on v5

--- a/solution.py
+++ b/solution.py
@@ -266,13 +266,13 @@
         pg(k).wait_recv()
 
         def take(cols, r):
-            acc[k, :, cols] = r
+            acc[(k + 1) % NZ, :, cols] = r
 
         expert(k, pair_sources, w, y % 2, take)
 
     def p_c(k):
         def take(cols, r):
-            o[k, 0:2, :, cols] = (acc[k, :, cols] + r).astype(BF).reshape(2, ROWS, 256)
+            o[k, 0:2, :, cols] = (acc[(k + 1) % NZ, :, cols] + r).astype(BF).reshape(2, ROWS, 256)
 
         expert(k, pair_sources, w2, 1 - y % 2, take)
         pr(k).start()
@@ -387,15 +387,13 @@
     with jax.named_scope("pair"):
         pair.wait_recv()
 
-    def join(e, carry):
-        mine, theirs = pieces[c, e], other[e]
-        low = jnp.where(c == 0, mine, theirs)
-        high = jnp.where(c == 0, theirs, mine)
-        wsend[e] = jnp.concatenate([low, high], axis=-1)
-        return carry
-
-    with jax.named_scope("join"):
-        lax.fori_loop(0, NZ * FINE, join, 0, unroll=4)
+    def join(s):
+        for n in range(FINE):
+            e = FINE * to_z(s) + n
+            mine, theirs = pieces[c, e], other[e]
+            low = jnp.where(c == 0, mine, theirs)
+            high = jnp.where(c == 0, theirs, mine)
+            wsend[e] = jnp.concatenate([low, high], axis=-1)
 
     def send(copy, first, last):
         def one(s, carry):
@@ -405,6 +403,7 @@
         lax.fori_loop(first, last, one, 0)
 
     def send_w(s):
+        join(s)
         for k in (1, 3, 2, 0):
             ws(s, k).start()
 
@@ -413,6 +412,7 @@
         for j in range(NY):
             wt(k, j).start()
 
+    join(0)
     for k in (1, 3, 2):
         ws(0, k, "ws0").start()
     w[:, x, NY * z + y, c] = wsend[FINE * z + y]
@@ -445,11 +445,11 @@
         pl.when(i < NZ - 2)(lambda: run(w_b, i + 2))
         pl.when(i < NZ)(lambda: run(w_c, i))
         pl.when(i >= 2)(lambda: run(w_d, i - 2))
-        at(i, 5, (t_a, 4), (p_a, 3))
+        at(i, 5, (t_a, 3), (t_a, 4))
         at(i, 6, (v_b, 0))
-        at(i, 7, (v_b, 1))
-        at(i, 8, (v_b, 2), (t_b, 4))
-        at(i, 9, (t_a, 5), (t_a, 6))
+        at(i, 7, (v_b, 1), (t_b, 3))
+        at(i, 8, (v_b, 2), (v_b, 3), (t_b, 4))
+        at(i, 9, (v_b, 4), (t_a, 5), (t_a, 6))
         return carry
 
     lax.fori_loop(0, NZ + 2, w_loop, 0)
@@ -461,21 +461,22 @@
         return carry
 
     def t_loop(i, carry):
-        run(t_c, i + PAIRED)
+        at(i, 2, (t_d, 4))
+        run(t_c, i + 3)
 
         @pl.when(i == 0)
         def _():
-            lax.fori_loop(3, NZ, v_start, 0)
-
-        at(i, 0, (v_c, 0), (v_c, 1))
-        run(p_b, (i + 1) % PAIRED)
-        at(i, 0, (t_b, 5), (v_c, 2), (t_b, 6), (t_a, 7), (t_d, 4), (v_c, 3))
-        at(i, 1, (v_c, 4))
-        at(i, 2, (v_c, 5), (t_b, 7), (t_e, 4), (v_c, 6), (t_d, 5), (v_d, 0), (v_d, 1), (t_d, 6))
-        at(
-            i, 3, (v_c, 7), (v_d, 2), (t_e, 5), (v_d, 3), (v_d, 4), (t_e, 6), (v_d, 5),
-            (t_d, 7), (v_d, 6), (v_d, 7),
-        )
+            lax.fori_loop(5, NZ, v_start, 0)
+
+        at(i, 0, (v_c, 0))
+        at(i, 1, (v_c, 1))
+        at(i, 3, (v_c, 6), (t_e, 3))
+        pl.when(i >= 1)(lambda: run(p_b, i % 3))
+        at(i, 1, (t_b, 5), (v_c, 2), (t_b, 6), (t_d, 3), (v_c, 3))
+        at(i, 2, (v_c, 4), (v_c, 5))
+        at(i, 3, (v_c, 7), (t_d, 5), (v_d, 0), (t_e, 4), (t_d, 6), (p_a, 7))
+        at(i, 3, *((v_d, k) for k in range(1, NZ)))
+        at(i, 3, (t_e, 5))
         return carry
 
     lax.fori_loop(0, NZ - PAIRED, t_loop, 0)
@@ -483,16 +484,21 @@
         arrived(w2.at[:, :, :, 0], cv_r)
 
     def p_at(i):
-        return i % 3 + 3 * ((3 - i) // 3)
+        return (i + 1) % 4 + 4 * ((i // 2) * (3 - i))
 
     def p_loop(i, carry):
         run(p_c, p_at(i))
-        at(i, 1, (t_e, 7))
-        pl.when(i >= 1)(lambda: run(p_e, p_at(i - 1)))
+        at(i, 0, (t_e, 6))
+        at(i, 1, (p_b, 7))
         return carry
 
     lax.fori_loop(0, PAIRED, p_loop, 0)
-    run(p_e, 0)
+
+    def e_loop(i, carry):
+        run(p_e, p_at(i))
+        return carry
+
+    lax.fori_loop(0, PAIRED, e_loop, 0)
     back[z] = zsum[0]
     many = NZ - 1
     all_sent(pieces.at[0], "pair")
@@ -506,8 +512,8 @@
     all_sent(w2.at[:, pl.ds(0, 3), :, 0], "xv")
     all_sent(w.at[:, :, :, 0], "cw")
     all_sent(w2.at[:, :, :, 0], "cv")
-    all_sent(a.at[pl.ds(PAIRED, NZ - PAIRED), pl.ds(0, 3)], "ag")
-    all_sent(o.at[pl.ds(PAIRED, NZ - PAIRED), pl.ds(0, 3)], "rs")
+    all_sent(a.at[pl.ds(0, NZ - PAIRED), pl.ds(0, 3)], "ag")
+    all_sent(o.at[pl.ds(0, NZ - PAIRED), pl.ds(0, 3)], "rs")
     all_sent(a.at[pl.ds(0, PAIRED), 0], "pg")
     all_sent(o.at[pl.ds(0, PAIRED), 0], "pr")
     with jax.named_scope("finish"):
@@ -570,7 +576,7 @@
         dma((8,)), dma((len(SENT),)),
         dma, dma, dma, dma,
         dma((NZ,)), dma((NZ,)), dma((NZ,)), dma((NZ,)),
-        dma((PAIRED,)), dma((PAIRED,)),
+        dma((NZ,)), dma((NZ,)),
         dma((NZ,)), dma((NZ,)),
         dma((NZ, 3)), dma((NZ, 3)), dma((NZ, 3)),
     ]

time: 107 us -> 105 us (0.981)
  Pallas kernels: 106 us -> 104 us
    pallas_call x1, Pallas kernels: 103 us -> 101 us  [exchange(): pl.pallas_call(kernel, out_shape=(pltpu.VMEM((NZ, ROWS, D), BF), pltpu.VM...]
where the time goes in v6:
time: 105 us; the launch traced here: 104 us
  Pallas kernels  104 us (99%)
    pallas_call x1, Pallas kernels, exchange(): pl.pallas_call(kernel, out_shape=(pltpu.VMEM((NZ, ROWS, D), BF), pltpu.VM...  101 us
    pallas_call x1, Pallas kernels, exchange(): pl.pallas_call(settle, out_shape=(jax.ShapeDtypeStruct((count, D), BF), r...  3.18 us

profile of v6, /device:TPU:1, one launch (start us, length us, event | category | flops | bytes accessed | tf_op | source)
XLA Modules:
  0.0 104.4 jit_solution(3540749185786171106)
XLA Ops:
  0.6 0.0 copy-start
  0.6 100.5 %shard_map.111 = (bf16[8,32,2048]{2,1,0:T(8,128)(2,1)S(1)}, bf16[3,4,32,2,32,128]{5,4,3,2,1,0:T(8,128)(2,1)S(1)}) custom-call(bf16[256,2048]{1,0:T(8,128)(2,1)} %tokens_in.1, s32[1,256]{1,0:T(1,128)} %bitcast.9, s32[2,256]{1,0:T(2,128)} %bitcast.11, f32[2,256]{1,0:T(2,128)} %bitcast.12, f32[1,64]{1,0:T(1,128)} %bitcast.13, f32[32,64,64]{2,1,0:T(8,128)} %gate_in.1, ...), custom_call_target="tpu_custom_call" | custom-call | tf_op jit(solution)/shard_map/pallas_call | solution.py:583
  101.2 0.0 copy-done
  101.2 3.2 %shard_map.112 = (bf16[256,2048]{1,0:T(8,128)(2,1)}, bf16[32,2,32,512]{3,2,1,0:T(8,128)(2,1)}, bf16[32,2,32,512]{3,2,1,0:T(8,128)(2,1)}, bf16[32,2,32,512]{3,2,1,0:T(8,128)(2,1)}) custom-call(bf16[256,2048]{1,0:T(8,128)(2,1)S(1)} %bitcast.8, bf16[3,4,32,2,32,128]{5,4,3,2,1,0:T(8,128)(2,1)S(1)} %get-tuple-element.11.w, s32[1,256]{1,0:T(1,128)S(1)} %bitcast.10), custom_call_target="tpu_custom_call" | custom-call | tf_op jit(solution)/shard_map/pallas_call | solution.py:596
Async XLA Ops:
  0.6 100.5 %copy-start = (s32[256]{0:T(256)S(1)}, s32[256]{0:T(256)}, u32[]{:S(2)}) copy-start(s32[256]{0:T(256)} %param.9) | copy-start | bytes 3076

commit v7 on v6

--- a/solution.py
+++ b/solution.py
@@ -99,7 +99,7 @@
             src, dst, where = a.at[s, 1, pl.ds(0, HALF)], a.at[s, 2, pl.ds(0, HALF)], yp
         else:
             src, dst, where = a.at[s, 3, pl.ds(HALF, HALF)], a.at[s, 2, pl.ds(HALF, HALF)], ym
-        return remote(src, dst, sem_of("ag"), ag_r.at[s, min(j, 2)], {"y": where})
+        return remote(src, dst, sem_of("ag"), ag_r.at[s - 3, min(j, 2)], {"y": where})
 
     def sw(s):
         rows = pl.ds(NY * from_z(s), NY)
@@ -138,10 +138,10 @@
 
     def pg(k):
         src = rows_in.at[z] if isinstance(k, int) and k == 0 else a.at[k, 0]
-        return remote(src, a.at[k, 1], sem_of("pg"), pg_r.at[k], {"y": partner})
+        return remote(src, a.at[k, 1], sem_of("pg"), pg_r.at[(k + 1) % NZ], {"y": partner})
 
     def pr(k):
-        return remote(o.at[k, 1], f.at[k, 0], sem_of("pr"), pr_r.at[k], {"y": partner})
+        return remote(o.at[k, 1], f.at[k, 0], sem_of("pr"), pr_r.at[(k + 1) % NZ], {"y": partner})
 
     def rs(s, j):
         if j == 0:
@@ -152,7 +152,7 @@
             src, dst, rr, where = o.at[s, 1], f.at[s, 0], f_r, ym
         else:
             src, dst, rr, where = o.at[s, 3], f.at[s, 1], f_r, yp
-        return remote(src, dst, sem_of("rs"), rr.at[s], {"y": where})
+        return remote(src, dst, sem_of("rs"), rr.at[s - 3], {"y": where})
 
     def zb(s):
         return remote(zsum.at[s], back.at[z], sem_of("zb"), zb_r, {"z": from_z(s)})
@@ -250,7 +250,7 @@
 
     def t_c(s):
         arrived(near.at[s], wt_r.at[s])
-        arrived(a.at[s, 2], ag_r.at[s, 2])
+        arrived(a.at[s, 2], ag_r.at[s - 3, 2])
 
         def take(cols, r):
             o[s, :, :, cols] = r.astype(BF).reshape(NY, ROWS, 256)
@@ -283,14 +283,14 @@
         pl.when(k > 0)(lambda: zb(k).start())
 
     def t_d(s):
-        arrived(h.at[s], h_r.at[s])
+        arrived(h.at[s], h_r.at[s - 3])
         o[s, 1, 0:HALF] = (o[s, 1, 0:HALF].astype(F32) + h[s, 0].astype(F32)).astype(BF)
         rs(s, 2).start()
         o[s, 3, HALF:ROWS] = (o[s, 3, HALF:ROWS].astype(F32) + h[s, 1].astype(F32)).astype(BF)
         rs(s, 3).start()
 
     def t_e(s):
-        arrived(f.at[s], f_r.at[s])
+        arrived(f.at[s], f_r.at[s - 3])
         zsum[s] = (
             o[s, 0].astype(F32) + f[s, 0].astype(F32) + f[s, 1].astype(F32)
         ).astype(BF)
@@ -461,7 +461,7 @@
         return carry
 
     def t_loop(i, carry):
-        at(i, 2, (t_d, 4))
+        at(i, 1, (v_c, 1), (p_b, 1), (t_b, 5), (v_c, 2))
         run(t_c, i + 3)
 
         @pl.when(i == 0)
@@ -469,13 +469,13 @@
             lax.fori_loop(5, NZ, v_start, 0)
 
         at(i, 0, (v_c, 0))
-        at(i, 1, (v_c, 1))
+        at(i, 1, (t_b, 6), (t_d, 3), (v_c, 3))
+        at(i, 2, (t_d, 4), (v_c, 4))
         at(i, 3, (v_c, 6), (t_e, 3))
-        pl.when(i >= 1)(lambda: run(p_b, i % 3))
-        at(i, 1, (t_b, 5), (v_c, 2), (t_b, 6), (t_d, 3), (v_c, 3))
-        at(i, 2, (v_c, 4), (v_c, 5))
-        at(i, 3, (v_c, 7), (t_d, 5), (v_d, 0), (t_e, 4), (t_d, 6), (p_a, 7))
-        at(i, 3, *((v_d, k) for k in range(1, NZ)))
+        pl.when(i >= 2)(lambda: run(p_b, (4 - 2 * (i - 1)) % 4))
+        at(i, 2, (v_c, 5))
+        at(i, 3, (v_c, 7), (t_d, 5), (v_d, 0), (v_d, 1), (t_d, 6), (p_a, 7), (t_e, 4))
+        at(i, 3, *((v_d, k) for k in range(2, NZ)))
         at(i, 3, (t_e, 5))
         return carry
 
@@ -576,9 +576,9 @@
         dma((8,)), dma((len(SENT),)),
         dma, dma, dma, dma,
         dma((NZ,)), dma((NZ,)), dma((NZ,)), dma((NZ,)),
-        dma((NZ,)), dma((NZ,)),
-        dma((NZ,)), dma((NZ,)),
-        dma((NZ, 3)), dma((NZ, 3)), dma((NZ, 3)),
+        dma((PAIRED,)), dma((PAIRED,)),
+        dma((NZ - PAIRED,)), dma((NZ - PAIRED,)),
+        dma((NZ - PAIRED, 3)), dma((NZ, 3)), dma((NZ, 3)),
     ]
     back, w = pl.pallas_call(
         kernel,

time: 105 us -> 105 us (level); the launches traced: 104 us -> 103 us
  Pallas kernels: 104 us -> 102 us
    pallas_call x1, Pallas kernels: 101 us -> 99.2 us  [exchange(): pl.pallas_call(kernel, out_shape=(pltpu.VMEM((NZ, ROWS, D), BF), pltpu.VM...]
where the time goes in v7:
time: 105 us; the launch traced here: 103 us
  Pallas kernels  102 us (97%)
    pallas_call x1, Pallas kernels, exchange(): pl.pallas_call(kernel, out_shape=(pltpu.VMEM((NZ, ROWS, D), BF), pltpu.VM...  99.2 us
    pallas_call x1, Pallas kernels, exchange(): pl.pallas_call(settle, out_shape=(jax.ShapeDtypeStruct((count, D), BF), r...  3.18 us

profile of v7, /device:TPU:1, one launch (start us, length us, event | category | flops | bytes accessed | tf_op | source)
XLA Modules:
  0.0 103.0 jit_solution(3180850360637966369)
XLA Ops:
  0.6 0.0 copy-start
  0.6 99.2 %shard_map.111 = (bf16[8,32,2048]{2,1,0:T(8,128)(2,1)S(1)}, bf16[3,4,32,2,32,128]{5,4,3,2,1,0:T(8,128)(2,1)S(1)}) custom-call(bf16[256,2048]{1,0:T(8,128)(2,1)} %tokens_in.1, s32[1,256]{1,0:T(1,128)} %bitcast.9, s32[2,256]{1,0:T(2,128)} %bitcast.11, f32[2,256]{1,0:T(2,128)} %bitcast.12, f32[1,64]{1,0:T(1,128)} %bitcast.13, f32[32,64,64]{2,1,0:T(8,128)} %gate_in.1, ...), custom_call_target="tpu_custom_call" | custom-call | tf_op jit(solution)/shard_map/pallas_call | solution.py:583
  99.8 0.0 copy-done
  99.9 3.2 %shard_map.112 = (bf16[256,2048]{1,0:T(8,128)(2,1)}, bf16[32,2,32,512]{3,2,1,0:T(8,128)(2,1)}, bf16[32,2,32,512]{3,2,1,0:T(8,128)(2,1)}, bf16[32,2,32,512]{3,2,1,0:T(8,128)(2,1)}) custom-call(bf16[256,2048]{1,0:T(8,128)(2,1)S(1)} %bitcast.8, bf16[3,4,32,2,32,128]{5,4,3,2,1,0:T(8,128)(2,1)S(1)} %get-tuple-element.11.w, s32[1,256]{1,0:T(1,128)S(1)} %bitcast.10), custom_call_target="tpu_custom_call" | custom-call | tf_op jit(solution)/shard_map/pallas_call | solution.py:596
Async XLA Ops:
  0.6 99.2 %copy-start = (s32[256]{0:T(256)S(1)}, s32[256]{0:T(256)}, u32[]{:S(2)}) copy-start(s32[256]{0:T(256)} %param.9) | copy-start | bytes 3076
